TPU v7x, 512 devices: a whole 4x8x8 slice. The times are simulated.
512 devices in a mesh: ep: 128 (over z, y, core), tp: 4 (over x).
Axes of the slice: x: 4, y: 8, z: 8, core: 2. Of those that a mesh axis runs over, the one named last changes fastest.
Arguments:
- tokens: bfloat16 [256, 2048], P('ep'), may hold values from -6 to 6
- w_query: bfloat16 [2048, 512], P(None, 'tp'), may hold values from -0.125 to 0.125
- w_key: bfloat16 [2048, 512], P(None, 'tp'), may hold values from -0.125 to 0.125
- w_value: bfloat16 [2048, 512], P(None, 'tp'), may hold values from -0.125 to 0.125
- w_forget: bfloat16 [4, 2048], P('tp'), may hold values from -0.25 to 0.25
- w_output: bfloat16 [512, 2048], P('tp'), may hold values from -0.25 to 0.25
- cache_keys: bfloat16 [256, 4, 1024, 128], P('ep', 'tp'), may hold values from -1000 to 1000
- cache_values: bfloat16 [256, 4, 1024, 128], P('ep', 'tp'), may hold values from -6 to 6
- cache_gates: float32 [256, 4, 1024], P('ep', 'tp'), may hold values from -68 to 0, as said below
- lengths: int32 [256], P('ep'), may hold values from 2 to 1024, as said below
- ln1_gain: float32 [2048], replicated, may hold values from 0.4 to 6
- ln1_shift: float32 [2048], replicated, may hold values from -1.8 to 1.8
- gate_vector: bfloat16 [2048], replicated, may hold values from -0.125 to 0.125
- dense_gate: bfloat16 [2048, 8192], P(None, ('ep', 'tp')), may hold values from -0.125 to 0.125
- dense_up: bfloat16 [2048, 8192], P(None, ('ep', 'tp')), may hold values from -0.125 to 0.125
- dense_down: bfloat16 [8192, 2048], P(('ep', 'tp')), may hold values from -0.0625 to 0.0625
- expert_gate: bfloat16 [128, 2048, 512], P('ep', None, 'tp'), may hold values from -0.125 to 0.125
- expert_up: bfloat16 [128, 2048, 512], P('ep', None, 'tp'), may hold values from -0.125 to 0.125
- expert_down: bfloat16 [128, 512, 2048], P('ep', 'tp'), may hold values from -0.25 to 0.25
- expert_ids: int32 [256, 2], replicated, may hold values from 0 to 127, as said below
- expert_weights: float32 [256, 2], replicated, may hold values from 0.1 to 1
- ln2_gain: float32 [2048], P('tp'), may hold values from 0.1 to 1.9
- ln2_shift: float32 [2048], P('tp'), may hold values from -1.8 to 1.8
Outputs:
- mixed: bfloat16 [256, 2048], P('ep', 'tp')
Inputs may be any that keep to these rules, and one draw needn't show every extreme that they name: `expert_ids`: each row names 2 different experts, all of them within one group of 4 consecutive expert numbers. `lengths`: some sequence has all 1024 positions in use. `cache_gates`: each head's values do not rise along positions.
All inputs are finite; a program needn't handle non-finite values.
Results may differ from a plain program's by a relative error of at most 0.012.
Values may be sent and summed in bfloat16 or wider, within the bound.
No kernel may reach another device: no remote copies, remote signals or barrier semaphores. Data moves between devices by JAX's collectives and lax.ppermute only.
A program may use at most 64 MiB of HBM per device.

v0:
```python
import jax
import jax.numpy as jnp
from jax import lax
from jax.sharding import Mesh
from jax.sharding import PartitionSpec as P

EP = ("ep_0", "ep_1", "ep_2")
EP_TP = ("ep_0", "ep_1", "ep_2", "tp")


alpha_scale = 1.4142135623730951
norm_eps = 1e-05


def sent_to_all(array, axis):
    copies = jnp.broadcast_to(array, (lax.axis_size(axis), *array.shape))
    return lax.all_to_all(copies, axis, split_axis=0, concat_axis=0, tiled=True)


def of_everyone(array, axis):
    return sent_to_all(array, axis).sum(axis=0)


def together(arrays, axis):
    ends = [0]
    for a in arrays:
        ends.append(ends[-1] + a.size)
    so_far = of_everyone(jnp.concatenate([a.ravel() for a in arrays]), axis)
    return tuple((so_far[b:e].reshape(a.shape) for a, b, e in zip(arrays, ends, ends[1:])))


def of_everyone_2(array, axis):
    everything = sent_to_all(array, axis)
    return jnp.sum(everything.astype(jnp.float32), axis=0)


def laid_out(tiles, dim):
    dims = list(tiles.shape[1:])
    dims[dim] *= tiles.shape[0]
    return jnp.moveaxis(tiles, 0, dim).reshape(dims)


def whole_of(array, axes, dim):
    far, near = axes
    tiles = sent_to_all(sent_to_all(array, far), near)
    return laid_out(tiles.swapaxes(0, 1).reshape(-1, *array.shape), dim)


def in_blocks(array, dim, count):
    before, after = (array.shape[:dim], array.shape[dim + 1 :])
    return jnp.moveaxis(array.reshape(*before, count, -1, *after), dim, 0)


def summed_on_arrival(array, axis, dim):
    tiles = in_blocks(array, dim, lax.axis_size(axis))
    arrived = lax.all_to_all(tiles, axis, split_axis=0, concat_axis=0, tiled=True)
    return arrived.astype(jnp.float32).sum(axis=0)


def sum_in_two_steps(array, axes, dim):
    far, near = axes
    tiles = in_blocks(array, dim, lax.axis_size(far))
    nearer = summed_on_arrival(tiles, near, dim + 1)
    arrived = lax.all_to_all(
        nearer.astype(jnp.bfloat16), far, split_axis=0, concat_axis=0, tiled=True
    )
    return arrived.astype(jnp.float32).sum(axis=0)


def sent_and_summed(array, axis, dim):
    count = lax.axis_size(axis)
    tiles = lax.all_to_all(in_blocks(array, dim, count), axis, 0, 0, tiled=True)
    return jnp.sum(tiles, axis=0)


def local_norm(values_in, gain_vec, shift_vec):
    row_mean = jnp.mean(values_in, axis=-1, keepdims=True)
    row_var = jnp.mean(values_in * values_in, axis=-1, keepdims=True) - row_mean * row_mean
    return (values_in - row_mean) * lax.rsqrt(row_var + norm_eps) * gain_vec + shift_vec


def spread_norm(final_rows, gain_vec, shift_vec, full_width):
    sums = together((jnp.sum(final_rows, axis=1), jnp.sum(final_rows * final_rows, axis=1)), "tp")
    row_mean = sums[0] / full_width
    row_var = sums[1] / full_width - row_mean * row_mean
    scaled = (final_rows - row_mean[:, None]) * lax.rsqrt(row_var + norm_eps)[:, None]
    return scaled * gain_vec + shift_vec


def per_device(
    tokens,
    w_query,
    w_key,
    w_value,
    w_forget,
    w_output,
    cache_keys,
    cache_values,
    cache_gates,
    lengths,
    ln1_gain,
    ln1_shift,
    gate_vector,
    dense_gate,
    dense_up,
    dense_down,
    expert_gate,
    expert_up,
    expert_down,
    expert_ids,
    expert_weights,
    ln2_gain,
    ln2_shift,
):
    query_rows = jnp.dot(tokens, w_query, preferred_element_type=jnp.float32).astype(jnp.bfloat16)
    new_keys = jnp.dot(tokens, w_key, preferred_element_type=jnp.float32).astype(jnp.bfloat16)
    new_values = jnp.dot(tokens, w_value, preferred_element_type=jnp.float32).astype(jnp.bfloat16)
    forget_new = jax.nn.log_sigmoid(
        jnp.einsum("sd,hd->sh", tokens, w_forget, preferred_element_type=jnp.float32)
    )[:, 0]
    score_scale = query_rows.shape[1] ** (-0.5)
    key_block = cache_keys[:, 0]
    value_block = cache_values[:, 0]
    gate_block = cache_gates[:, 0]
    positions = lax.broadcasted_iota(jnp.int32, gate_block.shape, 1)
    last_gate = jnp.sum(jnp.where(positions == lengths[:, None] - 1, gate_block, 0.0), axis=1)
    decay_bias = (last_gate + forget_new)[:, None] - gate_block
    scores = (
        jnp.einsum("sd,spd->sp", query_rows, key_block, preferred_element_type=jnp.float32)
        * score_scale
    )
    scores = jnp.where(positions < lengths[:, None], scores + decay_bias, -jnp.inf)
    own_score = (
        jnp.sum(query_rows.astype(jnp.float32) * new_keys.astype(jnp.float32), axis=1) * score_scale
    )
    peak = jnp.maximum(jnp.max(scores, axis=1), own_score)
    exp_terms = jnp.exp(scores - peak[:, None])
    own_exp = jnp.exp(own_score - peak)
    denominator = jnp.sum(exp_terms, axis=1) + own_exp
    probs = (exp_terms / denominator[:, None]).astype(jnp.bfloat16)
    own_prob = (own_exp / denominator).astype(jnp.bfloat16)
    weighted = jnp.einsum("sp,spd->sd", probs, value_block, preferred_element_type=jnp.float32)
    weighted = weighted + own_prob.astype(jnp.float32)[:, None] * new_values.astype(jnp.float32)
    head_output = weighted.astype(jnp.bfloat16)
    head_term = jnp.dot(head_output, w_output, preferred_element_type=jnp.float32).astype(
        jnp.bfloat16
    )
    attention = of_everyone_2(head_term, "tp").astype(jnp.float32)
    hidden = local_norm(
        alpha_scale * tokens.astype(jnp.float32) + attention, ln1_gain, ln1_shift
    ).astype(jnp.bfloat16)
    expert_index = lax.axis_index(EP)
    gate_own = expert_gate[0]
    up_own = expert_up[0]
    down_own = expert_down[0]
    segment = whole_of(hidden, (("ep_0", "ep_1"), "ep_2"), 0)
    route_share = jnp.sum(jnp.where(expert_ids == expert_index, expert_weights, 0.0), axis=1)
    mixing = jax.nn.sigmoid(jnp.dot(segment, gate_vector, preferred_element_type=jnp.float32))
    dense_a = jnp.dot(segment, dense_gate, preferred_element_type=jnp.float32)
    dense_b = jnp.dot(segment, dense_up, preferred_element_type=jnp.float32)
    dense_hidden = (jax.nn.silu(dense_a) * dense_b * mixing[:, None]).astype(jnp.bfloat16)
    expert_a = jnp.dot(segment, gate_own, preferred_element_type=jnp.float32)
    expert_b = jnp.dot(segment, up_own, preferred_element_type=jnp.float32)
    expert_hidden = (jax.nn.silu(expert_a) * expert_b * route_share[:, None]).astype(jnp.bfloat16)
    terms = jnp.dot(dense_hidden, dense_down, preferred_element_type=jnp.float32) + jnp.dot(
        expert_hidden, down_own, preferred_element_type=jnp.float32
    )
    full_width = terms.shape[1]
    own_cols = ln2_gain.shape[0]
    own_hidden = lax.dynamic_slice_in_dim(
        hidden, lax.axis_index("tp") * own_cols, own_cols, 1
    ).astype(jnp.float32)
    owner_terms = sum_in_two_steps(terms.astype(jnp.bfloat16), (("ep_0", "ep_1"), "ep_2"), 0)
    branches = sent_and_summed(owner_terms, "tp", 1)
    final_rows = alpha_scale * own_hidden + branches
    return spread_norm(final_rows, ln2_gain, ln2_shift, full_width).astype(jnp.bfloat16)


def solution(mesh):
    torus = Mesh(mesh.devices.reshape(8, 8, 2, mesh.shape["tp"]), ("ep_0", "ep_1", "ep_2", "tp"))
    in_specs = (
        P(EP, None),
        P(None, "tp"),
        P(None, "tp"),
        P(None, "tp"),
        P("tp", None),
        P("tp", None),
        P(EP, "tp", None, None),
        P(EP, "tp", None, None),
        P(EP, "tp", None),
        P(EP),
        P(),
        P(),
        P(),
        P(None, EP_TP),
        P(None, EP_TP),
        P(EP_TP, None),
        P(EP, None, "tp"),
        P(EP, None, "tp"),
        P(EP, "tp", None),
        P(),
        P(),
        P("tp"),
        P("tp"),
    )
    out_specs = P(EP, "tp")
    return jax.shard_map(
        per_device, mesh=torus, in_specs=in_specs, out_specs=out_specs, check_vma=False
    )
```

profile of v0, /device:TPU:8, one launch (start us, length us, event | category | flops | bytes accessed | tf_op | source)
XLA Modules:
  0.0 119.0 jit_solution(4536306620749316825)
XLA Ops:
  0.0 0.8 broadcast_add_fusion
  0.8 1.2 %convolution_convert_fusion.3 = bf16[2,128]{1,0:T(2,128)(2,1)S(1)} fusion(bf16[2,2048]{1,0:T(2,128)(2,1)} %param.23, bf16[2048,128]{1,0:T(8,128)(2,1)} %param.24), kind=kOutput, calls=%fused_computation.19 | convolution fusion | flops 1048832 | bytes 532992 | tf_op jit(solution)/shard_map/dot_general | solution.py:115
  2.0 1.4 %fusion.12 = f32[2]{0:T(128)S(1)} fusion(bf16[2,2048]{1,0:T(2,128)(2,1)} %param.23, bf16[2048,128]{1,0:T(8,128)(2,1)} %param.25, bf16[2,128]{1,0:T(2,128)(2,1)S(1)} %convolution_convert_fusion.3), kind=kOutput, calls=%fused_computation.18 | convolution fusion | flops 1049854 | bytes 533000 | tf_op jit(solution)/shard_map/dot_general | solution.py:116
  3.4 0.9 fusion.35
  4.3 0.9 fusion.46
  5.2 1.3 %fusion.21 = f32[2,1,1024]{2,1,0:T(1,128)S(1)} fusion(bf16[2,1,1024,128]{3,2,1,0:T(8,128)(2,1)} %param.29, bf16[2,128,1]{1,0,2:T(2,128)(2,1)S(1)} %bitcast.74), kind=kOutput, calls=%fused_computation.30 | convolution fusion | flops 524288 | bytes 532992 | tf_op jit(solution)/shard_map/sd,spd->sp/dot_general | solution.py:129
  6.5 0.9 fusion.55
  7.7 1.2 %fusion.19 = f32[2,1,128]{2,1,0:T(1,128)S(1)} fusion(bf16[2,1,1024,128]{3,2,1,0:T(8,128)(2,1)} %param.30, bf16[2,1024,1]{1,0,2:T(2,128)(2,1)S(1)} %fusion.42), kind=kOutput, calls=%fused_computation.28 | convolution fusion | flops 524288 | bytes 529408 | tf_op jit(solution)/shard_map/sp,spd->sd/dot_general | solution.py:142
  9.3 9.5 %all_to_all.36 = bf16[4,2,2048]{2,1,0:T(2,128)(2,1)S(1)} all-to-all(bf16[4,2,2048]{2,1,0:T(2,128)(2,1)S(1)} %broadcast_in_dim.21), channel_id=1, replica_groups=mesh['ep_0'=8,'ep_1'=8,'ep_2'=2,'tp'=4] {'tp'}, dimensions={0} | all-to-all | bytes 65536 | tf_op jit(solution)/shard_map/all_to_all | solution.py:17
  19.2 1.1 broadcast_in_dim.22
  20.3 16.6 %all-to-all-start.1 = ((bf16[64,2,2048]{2,1,0:T(2,128)(2,1)}), bf16[64,2,2048]{2,1,0:T(2,128)(2,1)S(1)}, u32[]{:S(2)}, u32[]{:S(2)}) async-start(bf16[64,2,2048]{2,1,0:T(2,128)(2,1)} %broadcast_in_dim.22), calls=%async_computation.1 | async-start | bytes 1048576 | tf_op jit(solution)/shard_map/all_to_all | solution.py:17
  37.0 17.9 %all-to-all-done.1 = bf16[64,2,2048]{2,1,0:T(2,128)(2,1)S(1)} async-done(((bf16[64,2,2048]{2,1,0:T(2,128)(2,1)}), bf16[64,2,2048]{2,1,0:T(2,128)(2,1)S(1)}, u32[]{:S(2)}, u32[]{:S(2)}) %all-to-all-start.1) | async-done | bytes 524320 | tf_op jit(solution)/shard_map/all_to_all | solution.py:17
  55.4 4.6 %all_to_all.37 = bf16[2,64,2,2048]{3,2,1,0:T(2,128)(2,1)S(1)} all-to-all(bf16[2,64,2,2048]{3,2,1,0:T(2,128)(2,1)S(1)} %broadcast_in_dim.23), channel_id=1, replica_groups=mesh['ep_0'=8,'ep_1'=8,'ep_2'=2,'tp'=4] {'ep_2'}, dimensions={0} | all-to-all | bytes 2097152 | tf_op jit(solution)/shard_map/all_to_all | solution.py:17
  60.0 1.2 %copy.36 = bf16[64,2,2,2048]{3,2,1,0:T(2,128)(2,1)S(1)} copy(bf16[64,2,2,2048]{3,2,0,1:T(2,128)(2,1)S(1)} %bitcast.71) | data formatting | bytes 2097152 | tf_op jit(solution)/shard_map/transpose | solution.py:46
  63.0 2.1 %fusion.3 = f32[256,2048]{1,0:T(8,128)} fusion(bf16[256,2048]{1,0:T(8,128)(2,1)S(1)} %reshape_reshape.6, bf16[1,128,2048]{2,1,0:T(8,128)(2,1)S(1)} %copy-done, bf16[1,2048,128]{2,1,0:T(8,128)(2,1)S(1)} %copy-done.1, f32[256,128]{1,0:T(8,128)S(1)} %fusion.17, f32[256]{0:T(256)S(1)} %fusion.43), kind=kOutput, calls=%fused_computation.6 | convolution fusion | flops 268664832 | bytes 4326400 | tf_op jit(solution)/shard_map/dot_general | solution.py:165
  65.1 3.0 %fusion = bf16[256,2048]{1,0:T(8,128)(2,1)S(1)} fusion(f32[256,2048]{1,0:T(8,128)} %fusion.3, bf16[16,2048]{1,0:T(8,128)(2,1)S(1)} %copy-done.6, bf16[256,2048]{1,0:T(8,128)(2,1)S(1)} %reshape_reshape.6, bf16[2048,16]{0,1:T(8,128)(2,1)S(1)} %copy-done.7, f32[256,16]{0,1:T(8,128)S(1)} %fusion.56, f32[256]{0:T(256)S(1)} %add_divide_fusion), kind=kOutput, calls=%fused_computation.1 | convolution fusion | flops 34631680 | bytes 4342784 | tf_op jit(solution)/shard_map/dot_general | solution.py:165
  68.8 0.7 copy.58
  69.5 4.6 %all_to_all.38 = bf16[2,64,2,2048]{3,2,1,0:T(2,128)(2,1)S(1)} all-to-all(bf16[2,64,2,2048]{3,2,1,0:T(2,128)(2,1)S(1)} %bitcast.72), channel_id=1, replica_groups=mesh['ep_0'=8,'ep_1'=8,'ep_2'=2,'tp'=4] {'ep_2'}, dimensions={0} | all-to-all | bytes 2097152 | tf_op jit(solution)/shard_map/all_to_all | solution.py:56
  74.1 2.3 %reduce_sum.127 = bf16[64,2,2048]{2,1,0:T(2,128)(2,1)S(1)} reduce(bf16[2,64,2,2048]{3,2,1,0:T(2,128)(2,1)S(1)} %all_to_all.38, bf16[]{:T(256)} %constant.60.clone.1), dimensions={0}, to_apply=%region_8.9 | reduce | flops 262144 | bytes 1572866 | tf_op jit(solution)/shard_map/reduce_sum | solution.py:57
  76.4 24.6 %all_to_all.39 = bf16[64,2,2048]{2,1,0:T(2,128)(2,1)S(1)} all-to-all(bf16[64,2,2048]{2,1,0:T(2,128)(2,1)S(1)} %reduce_sum.127), channel_id=1, replica_groups=mesh['ep_0'=8,'ep_1'=8,'ep_2'=2,'tp'=4] {'ep_0','ep_1'}, dimensions={0} | all-to-all | bytes 1048576 | tf_op jit(solution)/shard_map/all_to_all | solution.py:64
  101.0 0.8 convert_reduce_fusion
  101.8 3.2 %all-to-all-start.5 = ((f32[4,2,512]{2,1,0:T(2,128)}), f32[4,2,512]{2,1,0:T(2,128)S(1)}, u32[]{:S(2)}, u32[]{:S(2)}) async-start(f32[4,2,512]{2,1,0:T(2,128)} %bitcast.15), calls=%async_computation.5 | async-start | bytes 32768 | tf_op jit(solution)/shard_map/all_to_all | solution.py:72
  105.0 5.3 %all-to-all-done.5 = f32[4,2,512]{2,1,0:T(2,128)S(1)} async-done(((f32[4,2,512]{2,1,0:T(2,128)}), f32[4,2,512]{2,1,0:T(2,128)S(1)}, u32[]{:S(2)}, u32[]{:S(2)}) %all-to-all-start.5) | async-done | bytes 16416 | tf_op jit(solution)/shard_map/all_to_all | solution.py:72
  110.6 7.6 %all_to_all.40 = f32[4,1,4]{2,1,0:T(1,128)S(1)} all-to-all(f32[4,1,4]{2,1,0:T(1,128)S(1)} %broadcast_in_dim.45), channel_id=1, replica_groups=mesh['ep_0'=8,'ep_1'=8,'ep_2'=2,'tp'=4] {'tp'}, dimensions={0} | all-to-all | bytes 128 | tf_op jit(solution)/shard_map/all_to_all | solution.py:17
  (58 shorter events, 5.0 us)
Async XLA Ops:
  0.0 62.9 %copy-start = (bf16[1,128,2048]{2,1,0:T(8,128)(2,1)S(1)}, bf16[1,128,2048]{2,1,0:T(8,128)(2,1)}, u32[]{:S(2)}) copy-start(bf16[1,128,2048]{2,1,0:T(8,128)(2,1)} %param.41) | copy-start | bytes 1572868
  0.0 8.9 %copy-start.5 = (bf16[2,2048]{1,0:T(2,128)(2,1)S(1)}, bf16[2,2048]{1,0:T(2,128)(2,1)}, u32[]{:S(2)}) copy-start(bf16[2,2048]{1,0:T(2,128)(2,1)} %param.23) | copy-start | bytes 24580
  0.0 8.9 %copy-start.2 = (bf16[128,2048]{1,0:T(8,128)(2,1)S(1)}, bf16[128,2048]{1,0:T(8,128)(2,1)}, u32[]{:S(2)}) copy-start(bf16[128,2048]{1,0:T(8,128)(2,1)} %param.28) | copy-start | bytes 1572868
  0.0 8.9 %copy-start.3 = (bf16[2048,128]{1,0:T(8,128)(2,1)S(1)}, bf16[2048,128]{1,0:T(8,128)(2,1)}, u32[]{:S(2)}) copy-start(bf16[2048,128]{1,0:T(8,128)(2,1)} %param.26) | copy-start | bytes 1572868
  0.0 19.1 %copy-start.9 = (f32[2048]{0:T(1024)S(1)}, f32[2048]{0:T(1024)}, u32[]{:S(2)}) copy-start(f32[2048]{0:T(1024)} %param.34) | copy-start | bytes 24580
  0.0 19.1 %copy-start.10 = (f32[2048]{0:T(1024)S(1)}, f32[2048]{0:T(1024)}, u32[]{:S(2)}) copy-start(f32[2048]{0:T(1024)} %param.33) | copy-start | bytes 24580
  3.4 33.5 %copy-start.11 = (bf16[2048]{0:T(1024)(128)(2,1)S(1)}, bf16[2048]{0:T(1024)(128)(2,1)}, u32[]{:S(2)}) copy-start(bf16[2048]{0:T(1024)(128)(2,1)} %param.35) | copy-start | bytes 12292
  3.4 33.5 %copy-start.14 = (f32[256,2]{0,1:T(2,128)S(1)}, f32[256,2]{0,1:T(2,128)}, u32[]{:S(2)}) copy-start(f32[256,2]{0,1:T(2,128)} %param.43) | copy-start | bytes 6148
  3.4 33.5 %copy-start.15 = (s32[256,2]{0,1:T(2,128)S(1)}, s32[256,2]{0,1:T(2,128)}, u32[]{:S(2)}) copy-start(s32[256,2]{0,1:T(2,128)} %param.42) | copy-start | bytes 6148
  20.3 34.6 %all-to-all-start.1 = ((bf16[64,2,2048]{2,1,0:T(2,128)(2,1)}), bf16[64,2,2048]{2,1,0:T(2,128)(2,1)S(1)}, u32[]{:S(2)}, u32[]{:S(2)}) async-start(bf16[64,2,2048]{2,1,0:T(2,128)(2,1)} %broadcast_in_dim.22), calls=%async_computation.1 | async-start | bytes 1048576 | tf_op jit(solution)/shard_map/all_to_all | solution.py:17
  61.2 0.9 copy-start.8
  61.2 1.3 %copy-start.4 = (bf16[1,2048,128]{2,1,0:T(8,128)(2,1)S(1)}, bf16[1,2048,128]{2,1,0:T(8,128)(2,1)}, u32[]{:S(2)}) copy-start(bf16[1,2048,128]{2,1,0:T(8,128)(2,1)} %param.39) | copy-start | bytes 1572868
  61.7 1.3 %copy-start.1 = (bf16[1,2048,128]{2,1,0:T(8,128)(2,1)S(1)}, bf16[1,2048,128]{2,1,0:T(8,128)(2,1)}, u32[]{:S(2)}) copy-start(bf16[1,2048,128]{2,1,0:T(8,128)(2,1)} %param.40) | copy-start | bytes 1572868
  62.9 2.2 %copy-start.6 = (bf16[16,2048]{1,0:T(8,128)(2,1)S(1)}, bf16[16,2048]{1,0:T(8,128)(2,1)}, u32[]{:S(2)}) copy-start(bf16[16,2048]{1,0:T(8,128)(2,1)} %param.38) | copy-start | bytes 196612
  62.9 2.1 %copy-start.7 = (bf16[2048,16]{0,1:T(8,128)(2,1)S(1)}, bf16[2048,16]{0,1:T(8,128)(2,1)}, u32[]{:S(2)}) copy-start(bf16[2048,16]{0,1:T(8,128)(2,1)} %param.37) | copy-start | bytes 196612
  74.1 44.2 %copy-start.12 = (f32[512]{0:T(512)S(1)}, f32[512]{0:T(512)}, u32[]{:S(2)}) copy-start(f32[512]{0:T(512)} %param.45) | copy-start | bytes 6148
  74.1 44.2 %copy-start.13 = (f32[512]{0:T(512)S(1)}, f32[512]{0:T(512)}, u32[]{:S(2)}) copy-start(f32[512]{0:T(512)} %param.44) | copy-start | bytes 6148
  101.8 8.6 %all-to-all-start.5 = ((f32[4,2,512]{2,1,0:T(2,128)}), f32[4,2,512]{2,1,0:T(2,128)S(1)}, u32[]{:S(2)}, u32[]{:S(2)}) async-start(f32[4,2,512]{2,1,0:T(2,128)} %bitcast.15), calls=%async_computation.5 | async-start | bytes 32768 | tf_op jit(solution)/shard_map/all_to_all | solution.py:72
where the time goes:
time: 120 us; the launch traced here: 119 us
  blocking collectives  50.9 us (42%)
  waiting for transfers between devices  23.2 us (19%)
  starting transfers between devices  19.8 us (16%)
  matrix products  12.6 us (10%)
  other arithmetic  7.31 us (6%)
  local copies, waits for them, and re-layouts  4.82 us (4%)
    all_to_all x1, blocking collectives, sum_in_two_steps(): lax.all_to_all(nearer.astype(jnp.bfloat16), far, split_axis=0, concat_axi...  24.6 us
    all_to_all x3, blocking collectives, sent_to_all(): return lax.all_to_all(copies, axis, split_axis=0, concat_axis=0, tiled=True)  21.7 us
    all_to_all x1, waiting for transfers between devices, sent_to_all(): return lax.all_to_all(copies, axis, split_axis=0, concat_axis=0, tiled=True)  17.9 us
    all_to_all x1, starting transfers between devices, sent_to_all(): return lax.all_to_all(copies, axis, split_axis=0, concat_axis=0, tiled=True)  16.6 us
    all_to_all x1, waiting for transfers between devices, sent_and_summed(): tiles = lax.all_to_all(in_blocks(array, dim, count), axis, 0, 0, tiled=True)  5.32 us
    all_to_all x1, blocking collectives, summed_on_arrival(): lax.all_to_all(tiles, axis, split_axis=0, concat_axis=0, tiled=True)  4.58 us
    all_to_all x1, starting transfers between devices, sent_and_summed(): tiles = lax.all_to_all(in_blocks(array, dim, count), axis, 0, 0, tiled=True)  3.25 us
    dot_general x1, matrix products, per_device(): jnp.dot(dense_hidden, dense_down, preferred_element_type=jnp.float32)  2.96 us
  transfers between devices with their start and end apart: 2, of which 2 were waited for; matrix products, arithmetic and copies ran while one was open for 0% of the time, Pallas kernels for 0%

commit v1 on v0

v1 whole, which is shorter than its diff:
```python
import jax
import jax.numpy as jnp
from jax import lax
from jax.sharding import Mesh
from jax.sharding import PartitionSpec as P

EP = ("ep_0", "ep_1", "ep_2")
EP_TP = ("ep_0", "ep_1", "ep_2", "tp")


PLANE = ("ep_0", "ep_1")
OTHER_CORE = ((0, 1), (1, 0))

alpha_scale = 1.4142135623730951
norm_eps = 1e-05


def sent_to_all(array, axis):
    copies = jnp.broadcast_to(array, (lax.axis_size(axis), *array.shape))
    return lax.all_to_all(copies, axis, split_axis=0, concat_axis=0, tiled=True)


def of_everyone_2(array, axis):
    everything = sent_to_all(array, axis)
    return jnp.sum(everything.astype(jnp.float32), axis=0)


def in_blocks(array, dim, count):
    before, after = (array.shape[:dim], array.shape[dim + 1 :])
    return jnp.moveaxis(array.reshape(*before, count, -1, *after), dim, 0)


def summed_on_arrival(array, axis, dim):
    tiles = in_blocks(array, dim, lax.axis_size(axis))
    arrived = lax.all_to_all(tiles, axis, split_axis=0, concat_axis=0, tiled=True)
    return arrived.astype(jnp.float32).sum(axis=0)


def local_norm(values_in, gain_vec, shift_vec):
    row_mean = jnp.mean(values_in, axis=-1, keepdims=True)
    row_var = jnp.mean(values_in * values_in, axis=-1, keepdims=True) - row_mean * row_mean
    return (values_in - row_mean) * lax.rsqrt(row_var + norm_eps) * gain_vec + shift_vec


def branch_terms(
    rows, share, gate_vector, dense_gate, dense_up, dense_down, gate_own, up_own, down_own
):
    mixing = jax.nn.sigmoid(jnp.dot(rows, gate_vector, preferred_element_type=jnp.float32))
    dense_a = jnp.dot(rows, dense_gate, preferred_element_type=jnp.float32)
    dense_b = jnp.dot(rows, dense_up, preferred_element_type=jnp.float32)
    dense_hidden = (jax.nn.silu(dense_a) * dense_b * mixing[:, None]).astype(jnp.bfloat16)
    expert_a = jnp.dot(rows, gate_own, preferred_element_type=jnp.float32)
    expert_b = jnp.dot(rows, up_own, preferred_element_type=jnp.float32)
    expert_hidden = (jax.nn.silu(expert_a) * expert_b * share[:, None]).astype(jnp.bfloat16)
    return jnp.dot(dense_hidden, dense_down, preferred_element_type=jnp.float32) + jnp.dot(
        expert_hidden, down_own, preferred_element_type=jnp.float32
    )


def per_device(
    tokens,
    w_query,
    w_key,
    w_value,
    w_forget,
    w_output,
    cache_keys,
    cache_values,
    cache_gates,
    lengths,
    ln1_gain,
    ln1_shift,
    gate_vector,
    dense_gate,
    dense_up,
    dense_down,
    expert_gate,
    expert_up,
    expert_down,
    expert_ids,
    expert_weights,
    ln2_gain,
    ln2_shift,
):
    expert_index = lax.axis_index(EP)
    core = lax.axis_index("ep_2")
    route_share = jnp.sum(jnp.where(expert_ids == expert_index, expert_weights, 0.0), axis=1)
    by_core = route_share.reshape(-1, 2, tokens.shape[0])
    share_near = jnp.where(core == 0, by_core[:, 0], by_core[:, 1]).reshape(-1)
    share_far = jnp.where(core == 0, by_core[:, 1], by_core[:, 0]).reshape(-1)
    own_start = lax.axis_index("tp") * ln2_gain.shape[0]
    tokens, share_near, share_far, own_start = lax.optimization_barrier(
        (tokens, share_near, share_far, own_start)
    )
    query_rows = jnp.dot(tokens, w_query, preferred_element_type=jnp.float32).astype(jnp.bfloat16)
    new_keys = jnp.dot(tokens, w_key, preferred_element_type=jnp.float32).astype(jnp.bfloat16)
    new_values = jnp.dot(tokens, w_value, preferred_element_type=jnp.float32).astype(jnp.bfloat16)
    forget_new = jax.nn.log_sigmoid(
        jnp.einsum("sd,hd->sh", tokens, w_forget, preferred_element_type=jnp.float32)
    )[:, 0]
    score_scale = query_rows.shape[1] ** (-0.5)
    key_block = cache_keys[:, 0]
    value_block = cache_values[:, 0]
    gate_block = cache_gates[:, 0]
    positions = lax.broadcasted_iota(jnp.int32, gate_block.shape, 1)
    last_gate = jnp.sum(jnp.where(positions == lengths[:, None] - 1, gate_block, 0.0), axis=1)
    decay_bias = (last_gate + forget_new)[:, None] - gate_block
    scores = (
        jnp.einsum("sd,spd->sp", query_rows, key_block, preferred_element_type=jnp.float32)
        * score_scale
    )
    scores = jnp.where(positions < lengths[:, None], scores + decay_bias, -jnp.inf)
    own_score = (
        jnp.sum(query_rows.astype(jnp.float32) * new_keys.astype(jnp.float32), axis=1) * score_scale
    )
    peak = jnp.maximum(jnp.max(scores, axis=1), own_score)
    exp_terms = jnp.exp(scores - peak[:, None])
    own_exp = jnp.exp(own_score - peak)
    denominator = jnp.sum(exp_terms, axis=1) + own_exp
    probs = (exp_terms / denominator[:, None]).astype(jnp.bfloat16)
    own_prob = (own_exp / denominator).astype(jnp.bfloat16)
    weighted = jnp.einsum("sp,spd->sd", probs, value_block, preferred_element_type=jnp.float32)
    weighted = weighted + own_prob.astype(jnp.float32)[:, None] * new_values.astype(jnp.float32)
    head_output = weighted.astype(jnp.bfloat16)
    head_term = jnp.dot(head_output, w_output, preferred_element_type=jnp.float32).astype(
        jnp.bfloat16
    )
    attention = of_everyone_2(head_term, "tp").astype(jnp.float32)
    hidden = local_norm(
        alpha_scale * tokens.astype(jnp.float32) + attention, ln1_gain, ln1_shift
    ).astype(jnp.bfloat16)
    rows = sent_to_all(hidden, PLANE).reshape(-1, hidden.shape[1])
    rows_far = lax.ppermute(rows, "ep_2", OTHER_CORE)
    weights = (
        gate_vector,
        dense_gate,
        dense_up,
        dense_down,
        expert_gate[0],
        expert_up[0],
        expert_down[0],
    )
    terms_near = branch_terms(rows, share_near, *weights)
    terms_far = branch_terms(rows_far, share_far, *weights).astype(jnp.bfloat16)
    terms_here = lax.ppermute(terms_far, "ep_2", OTHER_CORE)
    terms = (terms_near + terms_here.astype(jnp.float32)).astype(jnp.bfloat16)
    owned = lax.optimization_barrier(summed_on_arrival(terms, PLANE, 0)).astype(jnp.bfloat16)
    branches = of_everyone_2(owned, "tp")
    final_rows = alpha_scale * hidden.astype(jnp.float32) + branches
    row_mean = jnp.mean(final_rows, axis=-1, keepdims=True)
    row_var = jnp.mean(final_rows * final_rows, axis=-1, keepdims=True) - row_mean * row_mean
    own_cols = ln2_gain.shape[0]
    own_rows = lax.dynamic_slice_in_dim(
        final_rows, own_start, own_cols, 1, allow_negative_indices=False
    )
    scaled = (own_rows - row_mean) * lax.rsqrt(row_var + norm_eps)
    return (scaled * ln2_gain + ln2_shift).astype(jnp.bfloat16)


def solution(mesh):
    torus = Mesh(mesh.devices.reshape(8, 8, 2, mesh.shape["tp"]), ("ep_0", "ep_1", "ep_2", "tp"))
    in_specs = (
        P(EP, None),
        P(None, "tp"),
        P(None, "tp"),
        P(None, "tp"),
        P("tp", None),
        P("tp", None),
        P(EP, "tp", None, None),
        P(EP, "tp", None, None),
        P(EP, "tp", None),
        P(EP),
        P(),
        P(),
        P(),
        P(None, EP_TP),
        P(None, EP_TP),
        P(EP_TP, None),
        P(EP, None, "tp"),
        P(EP, None, "tp"),
        P(EP, "tp", None),
        P(),
        P(),
        P("tp"),
        P("tp"),
    )
    out_specs = P(EP, "tp")
    return jax.shard_map(
        per_device, mesh=torus, in_specs=in_specs, out_specs=out_specs, check_vma=False
    )
```

time: 120 us -> 101 us (0.84)
  blocking collectives: 50.9 us -> 76.4 us
  waiting for transfers between devices: 23.2 us -> 2.3 us
  starting transfers between devices: 19.8 us -> 3.95 us
  other arithmetic: 7.31 us -> 4 us
  matrix products: 12.6 us -> 9.64 us
    all_to_all x3, blocking collectives: 21.7 us -> 51.8 us  [sent_to_all(): return lax.all_to_all(copies, axis, split_axis=0, concat_axis=0, tiled=True)]
    all_to_all x1 -> x0, blocking collectives: 24.6 us -> none  [sum_in_two_steps(): lax.all_to_all(nearer.astype(jnp.bfloat16), far, split_axis=0, concat_axi...]
    all_to_all x2 -> x0, waiting for transfers between devices: 23.2 us -> none  [the longest x1 17.9 us: sent_to_all(): return lax.all_to_all(copies, axis, split_axis=0, concat_axis=0, tiled=True)]
    all_to_all x1, blocking collectives: 4.58 us -> 24.6 us  [summed_on_arrival(): lax.all_to_all(tiles, axis, split_axis=0, concat_axis=0, tiled=True)]
    all_to_all x2 -> x0, starting transfers between devices: 19.8 us -> none  [the longest x1 16.6 us: sent_to_all(): return lax.all_to_all(copies, axis, split_axis=0, concat_axis=0, tiled=True)]
    ppermute x0 -> x2, starting transfers between devices: none -> 3.95 us  [the longest x1 2.03 us: per_device(): terms_here = lax.ppermute(terms_far, 'ep_2', OTHER_CORE)]
    unnamed x33 -> x41, local copies, waits for them, and re-layouts: 0.1 us -> 2.5 us
    ppermute x0 -> x2, waiting for transfers between devices: none -> 2.3 us  [the longest x1 1.6 us: per_device(): rows_far = lax.ppermute(rows, 'ep_2', OTHER_CORE)]
  transfers between devices with their start and end apart: 2 -> 2, of which waited for: 2 -> 2; matrix products, arithmetic and copies ran while one was open for 0% -> 2% of each run, Pallas kernels for 0% -> 0%
where the time goes in v1:
time: 101 us; the launch traced here: 100 us
  blocking collectives  76.4 us (76%)
  matrix products  9.64 us (10%)
  other arithmetic  4 us (4%)
  starting transfers between devices  3.95 us (4%)
  local copies, waits for them, and re-layouts  3.79 us (4%)
  waiting for transfers between devices  2.3 us (2%)
    all_to_all x3, blocking collectives, sent_to_all(): return lax.all_to_all(copies, axis, split_axis=0, concat_axis=0, tiled=True)  51.8 us
    all_to_all x1, blocking collectives, summed_on_arrival(): lax.all_to_all(tiles, axis, split_axis=0, concat_axis=0, tiled=True)  24.6 us
    dot_general x2, matrix products, branch_terms(): jnp.dot(expert_hidden, down_own, preferred_element_type=jnp.float32)  2.9 us
    unnamed x41, local copies, waits for them, and re-layouts  2.5 us
    ppermute x1, starting transfers between devices, per_device(): terms_here = lax.ppermute(terms_far, 'ep_2', OTHER_CORE)  2.03 us
  transfers between devices with their start and end apart: 2, of which 2 were waited for; matrix products, arithmetic and copies ran while one was open for 2% of the time, Pallas kernels for 0%

profile of v1, /device:TPU:8, one launch (start us, length us, event | category | flops | bytes accessed | tf_op | source)
XLA Modules:
  0.0 100.4 jit_solution(14042680302390592596)
XLA Ops:
  0.0 0.8 fusion.69
  1.5 0.7 broadcast_add_fusion
  2.1 1.3 %convolution_convert_fusion.3 = bf16[2,128]{1,0:T(2,128)(2,1)S(1)} fusion(bf16[2,2048]{1,0:T(2,128)(2,1)} %param.23, bf16[2048,128]{1,0:T(8,128)(2,1)} %param.24), kind=kOutput, calls=%fused_computation.20 | convolution fusion | flops 1048832 | bytes 532992 | tf_op jit(solution)/shard_map/dot_general | solution.py:95
  5.3 1.4 %convolution_convert_fusion = bf16[2,2048]{1,0:T(2,128)(2,1)S(1)} fusion(bf16[128,2048]{1,0:T(8,128)(2,1)S(1)} %copy-done.7, f32[2,128]{1,0:T(2,128)S(1)} %bitcast.104, bf16[2,2048]{1,0:T(2,128)(2,1)S(1)} %copy-done.11, bf16[2048,128]{1,0:T(8,128)(2,1)} %param.26, f32[2]{0:T(128)S(1)} %get-tuple-element.22), kind=kOutput, calls=%fused_computation.3 | convolution fusion | flops 2102528 | bytes 1065992 | tf_op jit(solution)/shard_map/dot_general | solution.py:125
  6.8 9.5 %all_to_all.20 = bf16[4,2,2048]{2,1,0:T(2,128)(2,1)S(1)} all-to-all(bf16[4,2,2048]{2,1,0:T(2,128)(2,1)S(1)} %broadcast_in_dim.20), channel_id=1, replica_groups=mesh['ep_0'=8,'ep_1'=8,'ep_2'=2,'tp'=4] {'tp'}, dimensions={0} | all-to-all | bytes 65536 | tf_op jit(solution)/shard_map/all_to_all | solution.py:20
  16.6 0.5 copy-done.14
  17.6 34.4 %all_to_all.21 = bf16[64,2,2048]{2,1,0:T(2,128)(2,1)S(1)} all-to-all(bf16[64,2,2048]{2,1,0:T(2,128)(2,1)S(1)} %broadcast_in_dim.21), channel_id=1, replica_groups=mesh['ep_0'=8,'ep_1'=8,'ep_2'=2,'tp'=4] {'ep_0','ep_1'}, dimensions={0} | all-to-all | bytes 1048576 | tf_op jit(solution)/shard_map/all_to_all | solution.py:20
  52.2 1.9 %collective-permute-start = (bf16[128,2048]{1,0:T(8,128)(2,1)S(1)}, bf16[128,2048]{1,0:T(8,128)(2,1)S(1)}, u32[]{:S(2)}, u32[]{:S(2)}) collective-permute-start(bf16[128,2048]{1,0:T(8,128)(2,1)S(1)} %reshape.109), channel_id=1, source_target_pairs={{0,4},{4,0},{1,5},{5,1},{2,6},{6,2},{3,7},{7,3},{8,12},{12,8},{9,1... | collective-permute-start | bytes 1572872 | tf_op jit(solution)/shard_map/ppermute | solution.py:133
  54.4 1.6 %collective-permute-done = bf16[128,2048]{1,0:T(8,128)(2,1)S(1)} collective-permute-done((bf16[128,2048]{1,0:T(8,128)(2,1)S(1)}, bf16[128,2048]{1,0:T(8,128)(2,1)S(1)}, u32[]{:S(2)}, u32[]{:S(2)}) %collective-permute-start) | collective-permute-done | bytes 524320 | tf_op jit(solution)/shard_map/ppermute | solution.py:133
  56.5 0.3 fusion.26
  56.8 0.5 copy-done.9
  57.4 0.8 fusion.63
  58.4 1.3 %fusion = bf16[128,2048]{1,0:T(8,128)(2,1)} fusion(f32[128,2048]{1,0:T(8,128)S(1)} %fusion.63, bf16[1,128,2048]{2,1,0:T(8,128)(2,1)S(1)} %copy-done, f32[128,128]{1,0:T(8,128)S(1)} %fusion.26, bf16[128,2048]{1,0:T(8,128)(2,1)S(1)} %collective-permute-done, bf16[1,2048,128]{2,1,0:T(8,128)(2,1)S(1)} %copy-done.1, f32[128]{0:T(128)S(1)} %select_n.42), kind=kOutput, calls=%fused_computation.2 | convolution fusion | flops 134856704 | bytes 3211776 | tf_op jit(solution)/shard_map/dot_general | solution.py:55
  59.7 2.0 %collective-permute-start.1 = (bf16[128,2048]{1,0:T(8,128)(2,1)}, bf16[128,2048]{1,0:T(8,128)(2,1)}, u32[]{:S(2)}, u32[]{:S(2)}) collective-permute-start(bf16[128,2048]{1,0:T(8,128)(2,1)} %fusion), channel_id=1, source_target_pairs={{0,4},{4,0},{1,5},{5,1},{2,6},{6,2},{3,7},{7,3},{8,12},{12,8},{9,1... | collective-permute-start | bytes 1572872 | tf_op jit(solution)/shard_map/ppermute | solution.py:145
  62.0 0.3 fusion.32
  62.4 0.8 fusion.5
  63.2 0.7 collective-permute-done.1
  63.9 1.6 %add_convert_fusion = bf16[128,2048]{1,0:T(8,128)(2,1)S(1)} fusion(bf16[128,2048]{1,0:T(8,128)(2,1)} %collective-permute-done.1, f32[128,2048]{1,0:T(8,128)S(1)} %fusion.5, bf16[1,128,2048]{2,1,0:T(8,128)(2,1)S(1)} %copy-done, bf16[128,2048]{1,0:T(8,128)(2,1)S(1)} %reshape.109, bf16[1,2048,128]{2,1,0:T(8,128)(2,1)S(1)} %copy-done.3, ...), kind=kOutput, calls=%fused_computation.34 | convolution fusion | flops 135380992 | bytes 3736064 | tf_op jit(solution)/shard_map/dot_general | solution.py:55
  65.5 0.3 reshape.110
  65.8 24.6 %all_to_all.22 = bf16[64,2,2048]{2,1,0:T(2,128)(2,1)S(1)} all-to-all(bf16[64,2,2048]{2,1,0:T(2,128)(2,1)S(1)} %reshape.110), channel_id=1, replica_groups=mesh['ep_0'=8,'ep_1'=8,'ep_2'=2,'tp'=4] {'ep_0','ep_1'}, dimensions={0} | all-to-all | bytes 1048576 | tf_op jit(solution)/shard_map/all_to_all | solution.py:35
  90.4 0.4 convert_reduce_fusion
  90.9 7.9 %all_to_all.23 = bf16[4,2,2048]{2,1,0:T(2,128)(2,1)S(1)} all-to-all(bf16[4,2,2048]{2,1,0:T(2,128)(2,1)S(1)} %broadcast_in_dim.22), channel_id=1, replica_groups=mesh['ep_0'=8,'ep_1'=8,'ep_2'=2,'tp'=4] {'tp'}, dimensions={0} | all-to-all | bytes 65536 | tf_op jit(solution)/shard_map/all_to_all | solution.py:20
  99.0 0.7 copy-done.17
  99.7 0.7 add_convert_fusion.2
  (67 shorter events, 5.0 us)
Async XLA Ops:
  0.0 58.2 %copy-start = (bf16[1,128,2048]{2,1,0:T(8,128)(2,1)S(1)}, bf16[1,128,2048]{2,1,0:T(8,128)(2,1)}, u32[]{:S(2)}) copy-start(bf16[1,128,2048]{2,1,0:T(8,128)(2,1)} %param.41) | copy-start | bytes 1572868
  0.0 3.4 %copy-start.4 = (bf16[2048,128]{1,0:T(8,128)(2,1)S(1)}, bf16[2048,128]{1,0:T(8,128)(2,1)}, u32[]{:S(2)}) copy-start(bf16[2048,128]{1,0:T(8,128)(2,1)} %param.25) | copy-start | bytes 1572868
  1.3 2.1 %copy-start.11 = (bf16[2,2048]{1,0:T(2,128)(2,1)S(1)}, bf16[2,2048]{1,0:T(2,128)(2,1)}, u32[]{:S(2)}) copy-start(bf16[2,2048]{1,0:T(2,128)(2,1)} %param.23) | copy-start | bytes 24580
  2.1 1.6 %copy-start.12 = (f32[2,1,1024]{2,1,0:T(1,128)S(1)}, f32[2,1,1024]{2,1,0:T(1,128)}, u32[]{:S(2)}) copy-start(f32[2,1,1024]{2,1,0:T(1,128)} %param.31) | copy-start | bytes 24580
  2.1 1.8 %copy-start.19 = (bf16[1,2048]{1,0:T(2,128)(2,1)S(1)}, bf16[1,2048]{1,0:T(2,128)(2,1)}, u32[]{:S(2)}) copy-start(bf16[1,2048]{1,0:T(2,128)(2,1)} %param.27) | copy-start | bytes 12292
  2.1 2.0 %copy-start.5 = (bf16[2,1,1024,128]{3,2,1,0:T(8,128)(2,1)S(1)}, bf16[2,1,1024,128]{3,2,1,0:T(8,128)(2,1)}, u32[]{:S(2)}) copy-start(bf16[2,1,1024,128]{3,2,1,0:T(8,128)(2,1)} %param.29) | copy-start | bytes 1572868
  3.5 1.7 %copy-start.6 = (bf16[2,1,1024,128]{3,2,1,0:T(8,128)(2,1)S(1)}, bf16[2,1,1024,128]{3,2,1,0:T(8,128)(2,1)}, u32[]{:S(2)}) copy-start(bf16[2,1,1024,128]{3,2,1,0:T(8,128)(2,1)} %param.30) | copy-start | bytes 1572868
  4.0 0.7 copy-start.18
  4.1 1.2 %copy-start.7 = (bf16[128,2048]{1,0:T(8,128)(2,1)S(1)}, bf16[128,2048]{1,0:T(8,128)(2,1)}, u32[]{:S(2)}) copy-start(bf16[128,2048]{1,0:T(8,128)(2,1)} %param.28) | copy-start | bytes 1572868
  16.4 0.7 copy-start.14
  16.5 0.7 copy-start.13
  52.0 2.1 %copy-start.15 = (bf16[2048]{0:T(1024)(128)(2,1)S(1)}, bf16[2048]{0:T(1024)(128)(2,1)}, u32[]{:S(2)}) copy-start(bf16[2048]{0:T(1024)(128)(2,1)} %param.35) | copy-start | bytes 12292
  52.0 2.2 %copy-start.8 = (bf16[2048,16]{0,1:T(8,128)(2,1)S(1)}, bf16[2048,16]{0,1:T(8,128)(2,1)}, u32[]{:S(2)}) copy-start(bf16[2048,16]{0,1:T(8,128)(2,1)} %param.36) | copy-start | bytes 196612
  52.2 3.8 %collective-permute-start = (bf16[128,2048]{1,0:T(8,128)(2,1)S(1)}, bf16[128,2048]{1,0:T(8,128)(2,1)S(1)}, u32[]{:S(2)}, u32[]{:S(2)}) collective-permute-start(bf16[128,2048]{1,0:T(8,128)(2,1)S(1)} %reshape.109), channel_id=1, source_target_pairs={{0,4},{4,0},{1,5},{5,1},{2,6},{6,2},{3,7},{7,3},{8,12},{12,8},{9,1... | collective-permute-start | bytes 1572872 | tf_op jit(solution)/shard_map/ppermute | solution.py:133
  54.4 2.1 %copy-start.2 = (bf16[1,2048,128]{2,1,0:T(8,128)(2,1)S(1)}, bf16[1,2048,128]{2,1,0:T(8,128)(2,1)}, u32[]{:S(2)}) copy-start(bf16[1,2048,128]{2,1,0:T(8,128)(2,1)} %param.40) | copy-start | bytes 1572868
  56.5 0.9 copy-start.9
  56.5 0.9 copy-start.10
  57.4 1.0 %copy-start.1 = (bf16[1,2048,128]{2,1,0:T(8,128)(2,1)S(1)}, bf16[1,2048,128]{2,1,0:T(8,128)(2,1)}, u32[]{:S(2)}) copy-start(bf16[1,2048,128]{2,1,0:T(8,128)(2,1)} %param.39) | copy-start | bytes 1572868
  59.7 4.1 %collective-permute-start.1 = (bf16[128,2048]{1,0:T(8,128)(2,1)}, bf16[128,2048]{1,0:T(8,128)(2,1)}, u32[]{:S(2)}, u32[]{:S(2)}) collective-permute-start(bf16[128,2048]{1,0:T(8,128)(2,1)} %fusion), channel_id=1, source_target_pairs={{0,4},{4,0},{1,5},{5,1},{2,6},{6,2},{3,7},{7,3},{8,12},{12,8},{9,1... | collective-permute-start | bytes 1572872 | tf_op jit(solution)/shard_map/ppermute | solution.py:145
  62.3 1.5 %copy-start.3 = (bf16[1,2048,128]{2,1,0:T(8,128)(2,1)S(1)}, bf16[1,2048,128]{2,1,0:T(8,128)(2,1)}, u32[]{:S(2)}) copy-start(bf16[1,2048,128]{2,1,0:T(8,128)(2,1)} %param.40) | copy-start | bytes 1572868
  99.0 0.7 copy-start.17
  99.0 0.7 copy-start.16

commit v2 on v1

v2 whole, which is shorter than its diff:
```python
import functools

import jax
import jax.numpy as jnp
from jax import lax
from jax.experimental import pallas as pl
from jax.experimental.pallas import tpu as pltpu
from jax.sharding import Mesh
from jax.sharding import PartitionSpec as P

EP = ("ep_0", "ep_1", "ep_2")
EP_TP = ("ep_0", "ep_1", "ep_2", "tp")
PLANE = ("ep_0", "ep_1")
OTHER_CORE = ((0, 1), (1, 0))

alpha_scale = 1.4142135623730951
norm_eps = 1e-05

F32 = jnp.float32
BF16 = jnp.bfloat16
ANY = pl.BlockSpec(memory_space=pl.ANY)
VMEM = pl.BlockSpec(memory_space=pltpu.VMEM)
SMEM = pl.BlockSpec(memory_space=pltpu.SMEM)
NT = (((1,), (1,)), ((), ()))


def dot(a, b):
    return jnp.dot(a, b, preferred_element_type=F32)


def dot_nt(a, b):
    return lax.dot_general(a, b, NT, preferred_element_type=F32)


def in_vmem(x):
    return pltpu.with_memory_space_constraint(x, pltpu.VMEM)


def params(mib):
    return pltpu.CompilerParams(vmem_limit_bytes=mib << 20)


def attend_kernel(
    lengths_hbm,
    tokens_hbm,
    w_forget_hbm,
    cache_gates_hbm,
    w_query,
    w_key,
    w_value,
    w_output,
    cache_keys,
    cache_values,
    *rest,
):
    kept = (len(rest) - 13) // 2
    sources, (terms, tokens, *places) = rest[:kept], rest[kept : 2 * kept + 2]
    scratch = rest[2 * kept + 2 :]
    lengths, w_forget, cache_gates, q_v, k_v, v_v, o_v, keys_v, values_v, sems, kept_sems = scratch
    moves = [
        pltpu.make_async_copy(src, dst, sems.at[i])
        for i, (src, dst) in enumerate(
            (
                (tokens_hbm, tokens),
                (w_forget_hbm, w_forget),
                (lengths_hbm, lengths),
                (cache_gates_hbm, cache_gates),
                (w_query, q_v),
                (w_key, k_v),
                (cache_keys, keys_v),
                (w_value, v_v),
                (cache_values, values_v),
                (w_output, o_v),
            )
        )
    ]
    kept_moves = [
        pltpu.make_async_copy(src, dst, kept_sems.at[i])
        for i, (src, dst) in enumerate(zip(sources, places))
    ]
    for move in moves + kept_moves:
        move.start()

    for move in moves[:4]:
        move.wait()
    x = tokens[...]
    scale = w_query.shape[1] ** (-0.5)
    length = cache_gates.shape[2]
    forget = jnp.sum(x.astype(F32) * w_forget[...].astype(F32), axis=1, keepdims=True)
    forget_new = jax.nn.log_sigmoid(forget)
    second = lax.broadcasted_iota(jnp.int32, (2, 1), 0) == 1
    used = jnp.where(second, lengths[1], lengths[0])
    gates = jnp.where(second, cache_gates[1], cache_gates[0])
    positions = lax.broadcasted_iota(jnp.int32, (2, length), 1)
    last_gate = jnp.sum(jnp.where(positions == used - 1, gates, 0.0), axis=1, keepdims=True)
    decay_bias = (last_gate + forget_new) - gates

    moves[4].wait()
    query = dot(x, q_v[...]).astype(BF16)
    moves[5].wait()
    new_key = dot(x, k_v[...]).astype(BF16)
    own_score = (
        jnp.sum(query.astype(F32) * new_key.astype(F32), axis=1, keepdims=True) * scale
    )
    moves[6].wait()
    scores = jnp.where(second, dot_nt(query, keys_v[1, 0]), dot_nt(query, keys_v[0, 0])) * scale
    scores = jnp.where(positions < used, scores + decay_bias, -jnp.inf)
    peak = jnp.maximum(jnp.max(scores, axis=1, keepdims=True), own_score)
    exp_terms = jnp.exp(scores - peak)
    own_exp = jnp.exp(own_score - peak)
    denominator = jnp.sum(exp_terms, axis=1, keepdims=True) + own_exp
    probs = (exp_terms / denominator).astype(BF16)
    own_prob = (own_exp / denominator).astype(BF16)
    moves[7].wait()
    new_value = dot(x, v_v[...]).astype(BF16)
    moves[8].wait()
    weighted = jnp.where(second, dot(probs, values_v[1, 0]), dot(probs, values_v[0, 0]))
    weighted = weighted + own_prob.astype(F32) * new_value.astype(F32)
    moves[9].wait()
    term = dot(weighted.astype(BF16), o_v[...]).astype(BF16)
    for i in range(terms.shape[0]):
        terms[i] = term
    for move in kept_moves:
        move.wait()


def attend(copies, operands, kept):
    operands = [pltpu.with_memory_space_constraint(a, pltpu.HBM) for a in (*operands, *kept)]
    lengths, tokens, w_forget, gates, w_query, w_key, w_value, w_output, keys, values = operands[:10]
    held = (w_forget, gates, w_query, w_key, w_value, w_output, keys, values)
    return pl.pallas_call(
        attend_kernel,
        out_shape=[pltpu.VMEM((copies, tokens.shape[0], w_output.shape[1]), BF16)]
        + [pltpu.VMEM(a.shape, a.dtype) for a in (tokens, *kept)],
        in_specs=[pl.BlockSpec(memory_space=pltpu.HBM)] * len(operands),
        out_specs=[VMEM] * (2 + len(kept)),
        scratch_shapes=[
            pltpu.SMEM(lengths.shape, jnp.int32),
            *(pltpu.VMEM(a.shape, a.dtype) for a in held),
            pltpu.SemaphoreType.DMA((10,)),
            pltpu.SemaphoreType.DMA((len(kept),)),
        ],
        compiler_params=params(12),
        name="attend",
    )(*operands)


def normed(rows, width):
    row_mean = jnp.sum(rows, axis=-1, keepdims=True) * (1.0 / width)
    row_var = jnp.sum(rows * rows, axis=-1, keepdims=True) * (1.0 / width) - row_mean * row_mean
    return (rows - row_mean) * lax.rsqrt(row_var + norm_eps)


def hidden_kernel(heads, tokens, gain, shift, copies):
    attention = heads[0].astype(F32)
    for i in range(1, heads.shape[0]):
        attention = attention + heads[i].astype(F32)
    rows = alpha_scale * tokens[...].astype(F32) + attention
    hidden = (normed(rows, rows.shape[1]) * gain[...] + shift[...]).astype(BF16)
    for i in range(copies.shape[0]):
        copies[i] = hidden


def hidden_copies(count, heads, tokens, gain, shift):
    return pl.pallas_call(
        hidden_kernel,
        out_shape=pltpu.VMEM((count, *tokens.shape), BF16),
        in_specs=[VMEM] * 4,
        out_specs=VMEM,
        compiler_params=params(4),
        name="hidden_copies",
    )(in_vmem(heads), tokens, in_vmem(gain), in_vmem(shift))


def unit_values(far, rows, gate_vector, gate, up, dense_gate, dense_up, ids, shares):
    tokens = ids.shape[1]
    core = lax.axis_index("ep_2")
    expert = (lax.axis_index("ep_0") * lax.axis_size("ep_1") + lax.axis_index("ep_1")) * 2 + core
    side = 1 - core if far else core
    picked = jnp.where(ids[...] == expert, shares[...], 0.0)
    share_row = picked[0:1] + picked[1:2]
    count = rows.shape[0]
    row = lax.broadcasted_iota(jnp.int32, (count, tokens), 0)
    column = lax.broadcasted_iota(jnp.int32, (count, tokens), 1)
    match = column == 4 * (row >> 1) + 2 * side + (row & 1)
    share = jnp.sum(jnp.where(match, share_row, 0.0), axis=1, keepdims=True)
    x = rows[...]
    a = dot(x, gate[...])
    b = dot(x, up[...])
    units = (a / (1.0 + jnp.exp(-a)) * b * share).astype(BF16)
    dense_a = dot_nt(x, dense_gate[...])
    dense_b = dot_nt(x, dense_up[...])
    gates = jnp.broadcast_to(gate_vector[...], dense_gate.shape)
    mixing = 1.0 / (1.0 + jnp.exp(-dot_nt(x, gates)))
    dense = (dense_a / (1.0 + jnp.exp(-dense_a)) * dense_b * mixing).astype(BF16)
    return units, dense


def units_kernel(rows, gate_vector, gate, up, dense_gate, dense_up, ids, shares, units, dense):
    units[...], dense[...] = unit_values(
        False, rows, gate_vector, gate, up, dense_gate, dense_up, ids, shares
    )


def branch_kernel(
    after, rows, gate_vector, gate, up, dense_gate, dense_up, ids, shares, down, dense_down, terms
):
    units, dense = unit_values(
        True, rows, gate_vector, gate, up, dense_gate, dense_up, ids, shares
    )
    terms[...] = (dot(units, down[...]) + dot(dense, dense_down[...])).astype(BF16)


def down_kernel(units, dense, down, dense_down, terms):
    terms[...] = dot(units[...], down[...]) + dot(dense[...], dense_down[...])


def estimate(rows, depth, columns):
    return pl.CostEstimate(
        flops=2 * rows * depth * columns, bytes_accessed=4096, transcendentals=0
    )


def near_units(rows, gate_vector, gate, up, dense_gate, *rest):
    count, depth = rows.shape
    args = (rows, gate_vector, gate, up, dense_gate, *rest)
    return pl.pallas_call(
        units_kernel,
        out_shape=[
            pltpu.VMEM((count, gate.shape[1]), BF16),
            pltpu.VMEM((count, dense_gate.shape[0]), BF16),
        ],
        in_specs=[VMEM] * len(args),
        out_specs=[VMEM] * 2,
        compiler_params=params(8),
        cost_estimate=estimate(count, depth, 512),
        name="near_units",
    )(*map(in_vmem, args))


def far_terms(after, rows, *weights):
    return pl.pallas_call(
        branch_kernel,
        out_shape=pltpu.VMEM(rows.shape, BF16),
        in_specs=[ANY] + [VMEM] * (1 + len(weights)),
        out_specs=VMEM,
        compiler_params=params(8),
        cost_estimate=estimate(*rows.shape, 1024),
        name="far_terms",
    )(*map(in_vmem, (after, rows, *weights)))


def near_terms(units, dense, down, dense_down):
    args = (units, dense, down, dense_down)
    return pl.pallas_call(
        down_kernel,
        out_shape=pltpu.VMEM((units.shape[0], down.shape[1]), F32),
        in_specs=[VMEM] * 4,
        out_specs=VMEM,
        compiler_params=params(8),
        cost_estimate=estimate(units.shape[0], 512, down.shape[1]),
        name="near_terms",
    )(*map(in_vmem, args))


def last_kernel(parts, hidden, gain, shift, out):
    branches = parts[0].astype(F32)
    for i in range(1, parts.shape[0]):
        branches = branches + parts[i].astype(F32)
    rows = alpha_scale * hidden[0].astype(F32) + branches
    rows = normed(rows, rows.shape[1])
    width = out.shape[1]
    place = lax.axis_index("tp")
    own = rows[:, :width]
    for i in range(1, rows.shape[1] // width):
        own = jnp.where(place == i, rows[:, i * width : (i + 1) * width], own)
    out[...] = (own * gain[...] + shift[...]).astype(BF16)


def last_norm(parts, hidden, gain, shift):
    return pl.pallas_call(
        last_kernel,
        out_shape=jax.ShapeDtypeStruct((hidden.shape[1], gain.shape[1]), BF16),
        grid=(1,),
        in_specs=[
            VMEM,
            pl.BlockSpec((1, *hidden.shape[1:]), lambda i: (0, 0, 0)),
            VMEM,
            VMEM,
        ],
        out_specs=pl.BlockSpec((hidden.shape[1], gain.shape[1]), lambda i: (0, 0)),
        compiler_params=params(4),
        name="last_norm",
    )(parts, hidden, gain, shift)


def to_all(copies, axis):
    return lax.all_to_all(copies, axis, split_axis=0, concat_axis=0, tiled=True)


def per_device(
    tokens,
    w_query,
    w_key,
    w_value,
    w_forget,
    w_output,
    cache_keys,
    cache_values,
    cache_gates,
    lengths,
    ln1_gain,
    ln1_shift,
    gate_vector,
    dense_gate,
    dense_up,
    dense_down,
    expert_gate,
    expert_up,
    expert_down,
    expert_ids,
    expert_weights,
    ln2_gain,
    ln2_shift,
):
    kept = (
        expert_gate[0],
        expert_up[0],
        dense_gate.T,
        dense_up.T,
        expert_ids.T,
        expert_weights.T,
        expert_down[0],
        dense_down,
        ln1_gain[None],
        ln1_shift[None],
        ln2_gain[None],
        ln2_shift[None],
    )
    operands = (
        lengths,
        tokens,
        w_forget,
        cache_gates,
        w_query,
        w_key,
        w_value,
        w_output,
        cache_keys,
        cache_values,
    )
    heads, tokens, *kept = attend(lax.axis_size("tp"), operands, kept)
    unit_weights, down_weights = (gate_vector[None], *kept[:6]), kept[6:8]
    gain_1, shift_1, gain_2, shift_2 = kept[8:]
    plane = lax.axis_size(PLANE)
    copies = hidden_copies(plane, to_all(heads, "tp"), tokens, gain_1, shift_1)
    rows = to_all(copies, PLANE).reshape(-1, tokens.shape[1])
    rows_far = lax.ppermute(rows, "ep_2", OTHER_CORE)
    units, dense = near_units(rows, *unit_weights)
    terms_far = far_terms(units, rows_far, *unit_weights, *down_weights)
    terms_here = lax.ppermute(terms_far, "ep_2", OTHER_CORE)
    terms = near_terms(units, dense, *down_weights) + terms_here.astype(F32)
    arrived = to_all(terms.astype(BF16).reshape(plane, -1, terms.shape[1]), PLANE)
    owned = lax.optimization_barrier(arrived.astype(F32).sum(axis=0)).astype(BF16)
    parts = to_all(jnp.broadcast_to(owned, (lax.axis_size("tp"), *owned.shape)), "tp")
    return last_norm(parts, copies, gain_2, shift_2)


def solution(mesh):
    torus = Mesh(mesh.devices.reshape(8, 8, 2, mesh.shape["tp"]), ("ep_0", "ep_1", "ep_2", "tp"))
    in_specs = (
        P(EP, None),
        P(None, "tp"),
        P(None, "tp"),
        P(None, "tp"),
        P("tp", None),
        P("tp", None),
        P(EP, "tp", None, None),
        P(EP, "tp", None, None),
        P(EP, "tp", None),
        P(EP),
        P(),
        P(),
        P(),
        P(None, EP_TP),
        P(None, EP_TP),
        P(EP_TP, None),
        P(EP, None, "tp"),
        P(EP, None, "tp"),
        P(EP, "tp", None),
        P(),
        P(),
        P("tp"),
        P("tp"),
    )
    out_specs = P(EP, "tp")
    return jax.shard_map(
        per_device, mesh=torus, in_specs=in_specs, out_specs=out_specs, check_vma=False
    )
```

time: 101 us -> 91.3 us (0.904)
  matrix products: 9.64 us -> 0 us
  Pallas kernels: 0 us -> 7.09 us
  other arithmetic: 4 us -> 0.55 us
  local copies, waits for them, and re-layouts: 3.79 us -> 0.57 us
    dot_general x16 -> x0, matrix products: 9.64 us -> none  [the longest x2 2.9 us: branch_terms(): jnp.dot(expert_hidden, down_own, preferred_element_type=jnp.float32)]
    pallas_call x0 -> x6, Pallas kernels: none -> 7.09 us  [the longest x1 3.26 us: attend(): pl.pallas_call(attend_kernel, out_shape=[pltpu.VMEM((copies, tokens.shape...]
    unnamed x41 -> x2, local copies, waits for them, and re-layouts: 2.5 us -> 0.01 us
    reduce_sum x8 -> x1, other arithmetic: 2.08 us -> 0.45 us  [per_device(): arrived.astype(F32).sum(axis=0)]
  transfers between devices with their start and end apart: 2 -> 2, of which waited for: 2 -> 2; matrix products, arithmetic and copies ran while one was open for 2% -> 0% of each run, Pallas kernels for 0% -> 1%
where the time goes in v2:
time: 91.3 us; the launch traced here: 91 us
  blocking collectives  76.4 us (84%)
  Pallas kernels  7.09 us (8%)
  starting transfers between devices  3.97 us (4%)
  waiting for transfers between devices  2.35 us (3%)
    all_to_all x4, blocking collectives, to_all(): return lax.all_to_all(copies, axis, split_axis=0, concat_axis=0, tiled=True)  76.4 us
    pallas_call x1, Pallas kernels, attend(): pl.pallas_call(attend_kernel, out_shape=[pltpu.VMEM((copies, tokens.shape...  3.26 us
    ppermute x1, starting transfers between devices, per_device(): terms_here = lax.ppermute(terms_far, 'ep_2', OTHER_CORE)  2.04 us
    ppermute x1, starting transfers between devices, per_device(): rows_far = lax.ppermute(rows, 'ep_2', OTHER_CORE)  1.92 us
  transfers between devices with their start and end apart: 2, of which 2 were waited for; matrix products, arithmetic and copies ran while one was open for 0% of the time, Pallas kernels for 1%

profile of v2, /device:TPU:8, one launch (start us, length us, event | category | flops | bytes accessed | tf_op | source)
XLA Modules:
  0.0 91.0 jit_solution(17388067131912997371)
XLA Ops:
  0.0 3.3 %attend.1 = (bf16[4,2,2048]{2,1,0:T(2,128)(2,1)S(1)}, bf16[2,2048]{1,0:T(2,128)(2,1)S(1)}, bf16[2048,128]{1,0:T(8,128)(2,1)S(1)}, bf16[2048,128]{1,0:T(8,128)(2,...) custom-call(s32[2]{0:T(128)} %lengths_hbm.1, ...), custom_call_target="tpu_custom_call" | custom-call | tf_op jit(solution)/shard_map/attend/pallas_call | solution.py:131
  3.3 9.5 %all_to_all.20.heads = bf16[4,2,2048]{2,1,0:T(2,128)(2,1)S(1)} all-to-all(bf16[4,2,2048]{2,1,0:T(2,128)(2,1)S(1)} %get-tuple-element.21), channel_id=1, replica_groups=mesh['ep_0'=8,'ep_1'=8,'ep_2'=2,'tp'=4] {'tp'}, dimensions={0} | all-to-all | bytes 65536 | tf_op jit(solution)/shard_map/all_to_all | solution.py:298
  12.8 0.2 hidden_copies.1.hidden
  13.0 34.4 %all_to_all.21 = bf16[64,2,2048]{2,1,0:T(2,128)(2,1)S(1)} all-to-all(bf16[64,2,2048]{2,1,0:T(2,128)(2,1)S(1)} %hidden_copies.1.hidden), channel_id=1, replica_groups=mesh['ep_0'=8,'ep_1'=8,'ep_2'=2,'tp'=4] {'ep_0','ep_1'}, dimensions={0} | all-to-all | bytes 1048576 | tf_op jit(solution)/shard_map/all_to_all | solution.py:298
  47.3 0.0 copy-start
  47.3 0.2 reshape.6.rows
  47.5 1.9 %collective-permute-start = (bf16[128,2048]{1,0:T(8,128)(2,1)S(1)}, bf16[128,2048]{1,0:T(8,128)(2,1)S(1)}, u32[]{:S(2)}, u32[]{:S(2)}) collective-permute-start(bf16[128,2048]{1,0:T(8,128)(2,1)S(1)} %reshape.6.rows), channel_id=1, source_target_pairs={{0,4},{4,0},{1,5},{5,1},{2,6},{6,2},{3,7},{7,3},{8,12},{12,8},{9,1... | collective-permute-start | bytes 1572872 | tf_op jit(solution)/shard_map/ppermute | solution.py:358
  49.5 0.0 copy-done
  49.5 0.8 near_units.1
  50.3 1.0 %collective-permute-done.rows = bf16[128,2048]{1,0:T(8,128)(2,1)S(1)} collective-permute-done((bf16[128,2048]{1,0:T(8,128)(2,1)S(1)}, bf16[128,2048]{1,0:T(8,128)(2,1)S(1)}, u32[]{:S(2)}, u32[]{:S(2)}) %collective-permute-start) | collective-permute-done | bytes 524320 | tf_op jit(solution)/shard_map/ppermute | solution.py:358
  51.3 1.7 %far_terms.1 = bf16[128,2048]{1,0:T(8,128)(2,1)S(1)} custom-call(bf16[128,128]{1,0:T(8,128)(2,1)S(1)} %get-tuple-element.31.units.after, bf16[128,2048]{1,0:T(8,128)(2,1)S(1)} %collective-permute-done.rows, bf16[1,2048]{1,0:T(2,128)(2,1)S(1)} %broadcast_in_dim.22.gate_vector, bf16[2048,128]{1,0:T(8,128)(2,1)S(1)} %get-tuple-element.25.gate, ...), custom_call_target="tpu_custom_call" | custom-call | flops 536870912 | bytes 4096 | tf_op jit(solution)/shard_map/far_terms/pallas_call | solution.py:242
  53.1 2.0 %collective-permute-start.1 = (bf16[128,2048]{1,0:T(8,128)(2,1)S(1)}, bf16[128,2048]{1,0:T(8,128)(2,1)S(1)}, u32[]{:S(2)}, u32[]{:S(2)}) collective-permute-start(bf16[128,2048]{1,0:T(8,128)(2,1)S(1)} %far_terms.1), channel_id=1, source_target_pairs={{0,4},{4,0},{1,5},{5,1},{2,6},{6,2},{3,7},{7,3},{8,12},{12,8},{9,1... | collective-permute-start | bytes 1572872 | tf_op jit(solution)/shard_map/ppermute | solution.py:361
  55.1 0.4 near_terms.1
  55.5 1.4 %collective-permute-done.1 = bf16[128,2048]{1,0:T(8,128)(2,1)S(1)} collective-permute-done((bf16[128,2048]{1,0:T(8,128)(2,1)S(1)}, bf16[128,2048]{1,0:T(8,128)(2,1)S(1)}, u32[]{:S(2)}, u32[]{:S(2)}) %collective-permute-start.1) | collective-permute-done | bytes 524320 | tf_op jit(solution)/shard_map/ppermute | solution.py:361
  56.9 0.1 add_convert_fusion
  57.0 0.3 reshape.7
  57.3 24.6 %all_to_all.22 = bf16[64,2,2048]{2,1,0:T(2,128)(2,1)S(1)} all-to-all(bf16[64,2,2048]{2,1,0:T(2,128)(2,1)S(1)} %reshape.7), channel_id=1, replica_groups=mesh['ep_0'=8,'ep_1'=8,'ep_2'=2,'tp'=4] {'ep_0','ep_1'}, dimensions={0} | all-to-all | bytes 1048576 | tf_op jit(solution)/shard_map/all_to_all | solution.py:298
  82.0 0.4 convert_reduce_fusion
  82.4 7.9 %all_to_all.23.parts = bf16[4,2,2048]{2,1,0:T(2,128)(2,1)S(1)} all-to-all(bf16[4,2,2048]{2,1,0:T(2,128)(2,1)S(1)} %broadcast_in_dim.23), channel_id=1, replica_groups=mesh['ep_0'=8,'ep_1'=8,'ep_2'=2,'tp'=4] {'tp'}, dimensions={0} | all-to-all | bytes 65536 | tf_op jit(solution)/shard_map/all_to_all | solution.py:298
  90.3 0.7 last_norm.1
  (2 shorter events, 0.0 us)
Async XLA Ops:
  47.3 2.1 %copy-start = (bf16[2048]{0:T(1024)(128)(2,1)S(1)}, bf16[2048]{0:T(1024)(128)(2,1)}, u32[]{:S(2)}) copy-start(bf16[2048]{0:T(1024)(128)(2,1)} %param.35) | copy-start | bytes 12292
  47.5 3.8 %collective-permute-start = (bf16[128,2048]{1,0:T(8,128)(2,1)S(1)}, bf16[128,2048]{1,0:T(8,128)(2,1)S(1)}, u32[]{:S(2)}, u32[]{:S(2)}) collective-permute-start(bf16[128,2048]{1,0:T(8,128)(2,1)S(1)} %reshape.6.rows), channel_id=1, source_target_pairs={{0,4},{4,0},{1,5},{5,1},{2,6},{6,2},{3,7},{7,3},{8,12},{12,8},{9,1... | collective-permute-start | bytes 1572872 | tf_op jit(solution)/shard_map/ppermute | solution.py:358
  53.1 3.8 %collective-permute-start.1 = (bf16[128,2048]{1,0:T(8,128)(2,1)S(1)}, bf16[128,2048]{1,0:T(8,128)(2,1)S(1)}, u32[]{:S(2)}, u32[]{:S(2)}) collective-permute-start(bf16[128,2048]{1,0:T(8,128)(2,1)S(1)} %far_terms.1), channel_id=1, source_target_pairs={{0,4},{4,0},{1,5},{5,1},{2,6},{6,2},{3,7},{7,3},{8,12},{12,8},{9,1... | collective-permute-start | bytes 1572872 | tf_op jit(solution)/shard_map/ppermute | solution.py:361

commit v3 on v2

--- a/solution.py
+++ b/solution.py
@@ -53,10 +53,11 @@
     cache_values,
     *rest,
 ):
-    kept = (len(rest) - 13) // 2
-    sources, (terms, tokens, *places) = rest[:kept], rest[kept : 2 * kept + 2]
-    scratch = rest[2 * kept + 2 :]
+    kept = (len(rest) - 12) // 2
+    sources, (terms, tokens, *places) = rest[:kept], rest[kept : 2 * kept + 1]
+    scratch = rest[2 * kept + 1 :]
     lengths, w_forget, cache_gates, q_v, k_v, v_v, o_v, keys_v, values_v, sems, kept_sems = scratch
+    width = w_query.shape[1]
     moves = [
         pltpu.make_async_copy(src, dst, sems.at[i])
         for i, (src, dst) in enumerate(
@@ -66,17 +67,21 @@
                 (lengths_hbm, lengths),
                 (cache_gates_hbm, cache_gates),
                 (w_query, q_v),
+                (cache_keys, keys_v),
                 (w_key, k_v),
-                (cache_keys, keys_v),
+                (cache_values, values_v),
                 (w_value, v_v),
-                (cache_values, values_v),
                 (w_output, o_v),
             )
         )
     ]
+    targets = list(places)
+    dense_front = places[0]
+    rows = dense_front.shape[0] // 2
+    targets[:1] = (dense_front.at[:rows], dense_front.at[rows:])
     kept_moves = [
         pltpu.make_async_copy(src, dst, kept_sems.at[i])
-        for i, (src, dst) in enumerate(zip(sources, places))
+        for i, (src, dst) in enumerate(zip(sources, targets))
     ]
     for move in moves + kept_moves:
         move.start()
@@ -84,7 +89,7 @@
     for move in moves[:4]:
         move.wait()
     x = tokens[...]
-    scale = w_query.shape[1] ** (-0.5)
+    scale = width ** (-0.5)
     length = cache_gates.shape[2]
     forget = jnp.sum(x.astype(F32) * w_forget[...].astype(F32), axis=1, keepdims=True)
     forget_new = jax.nn.log_sigmoid(forget)
@@ -98,13 +103,13 @@
     moves[4].wait()
     query = dot(x, q_v[...]).astype(BF16)
     moves[5].wait()
+    scores = jnp.where(second, dot_nt(query, keys_v[1, 0]), dot_nt(query, keys_v[0, 0])) * scale
+    scores = jnp.where(positions < used, scores + decay_bias, -jnp.inf)
+    moves[6].wait()
     new_key = dot(x, k_v[...]).astype(BF16)
     own_score = (
         jnp.sum(query.astype(F32) * new_key.astype(F32), axis=1, keepdims=True) * scale
     )
-    moves[6].wait()
-    scores = jnp.where(second, dot_nt(query, keys_v[1, 0]), dot_nt(query, keys_v[0, 0])) * scale
-    scores = jnp.where(positions < used, scores + decay_bias, -jnp.inf)
     peak = jnp.maximum(jnp.max(scores, axis=1, keepdims=True), own_score)
     exp_terms = jnp.exp(scores - peak)
     own_exp = jnp.exp(own_score - peak)
@@ -112,9 +117,9 @@
     probs = (exp_terms / denominator).astype(BF16)
     own_prob = (own_exp / denominator).astype(BF16)
     moves[7].wait()
+    weighted = jnp.where(second, dot(probs, values_v[1, 0]), dot(probs, values_v[0, 0]))
+    moves[8].wait()
     new_value = dot(x, v_v[...]).astype(BF16)
-    moves[8].wait()
-    weighted = jnp.where(second, dot(probs, values_v[1, 0]), dot(probs, values_v[0, 0]))
     weighted = weighted + own_prob.astype(F32) * new_value.astype(F32)
     moves[9].wait()
     term = dot(weighted.astype(BF16), o_v[...]).astype(BF16)
@@ -127,13 +132,17 @@
 def attend(copies, operands, kept):
     operands = [pltpu.with_memory_space_constraint(a, pltpu.HBM) for a in (*operands, *kept)]
     lengths, tokens, w_forget, gates, w_query, w_key, w_value, w_output, keys, values = operands[:10]
+    dense_gate, dense_up = kept[:2]
+    joined = ((2 * dense_gate.shape[0], dense_gate.shape[1]),)
     held = (w_forget, gates, w_query, w_key, w_value, w_output, keys, values)
     return pl.pallas_call(
         attend_kernel,
         out_shape=[pltpu.VMEM((copies, tokens.shape[0], w_output.shape[1]), BF16)]
-        + [pltpu.VMEM(a.shape, a.dtype) for a in (tokens, *kept)],
+        + [pltpu.VMEM(tokens.shape, BF16)]
+        + [pltpu.VMEM(shape, BF16) for shape in joined]
+        + [pltpu.VMEM(a.shape, a.dtype) for a in kept[2:]],
         in_specs=[pl.BlockSpec(memory_space=pltpu.HBM)] * len(operands),
-        out_specs=[VMEM] * (2 + len(kept)),
+        out_specs=[VMEM] * (len(kept) + 1),
         scratch_shapes=[
             pltpu.SMEM(lengths.shape, jnp.int32),
             *(pltpu.VMEM(a.shape, a.dtype) for a in held),
@@ -172,47 +181,79 @@
     )(in_vmem(heads), tokens, in_vmem(gain), in_vmem(shift))
 
 
-def unit_values(far, rows, gate_vector, gate, up, dense_gate, dense_up, ids, shares):
+def unit_values(far, rows, gate_vector, front, dense_front, ids, shares):
     tokens = ids.shape[1]
     core = lax.axis_index("ep_2")
     expert = (lax.axis_index("ep_0") * lax.axis_size("ep_1") + lax.axis_index("ep_1")) * 2 + core
     side = 1 - core if far else core
+    x = rows[...].reshape(-1, rows.shape[2])
+    count = x.shape[0]
+    both = [dot(x, w[...]) for w in front]
+    dense_both = dot_nt(x, dense_front[...])
     picked = jnp.where(ids[...] == expert, shares[...], 0.0)
     share_row = picked[0:1] + picked[1:2]
-    count = rows.shape[0]
     row = lax.broadcasted_iota(jnp.int32, (count, tokens), 0)
     column = lax.broadcasted_iota(jnp.int32, (count, tokens), 1)
     match = column == 4 * (row >> 1) + 2 * side + (row & 1)
     share = jnp.sum(jnp.where(match, share_row, 0.0), axis=1, keepdims=True)
-    x = rows[...]
-    a = dot(x, gate[...])
-    b = dot(x, up[...])
+    mixed = jnp.sum(x.astype(F32) * gate_vector[...].astype(F32), axis=1, keepdims=True)
+    mixing = 1.0 / (1.0 + jnp.exp(-mixed))
+    a, b = halves(both[0]) if len(both) == 1 else both
     units = (a / (1.0 + jnp.exp(-a)) * b * share).astype(BF16)
-    dense_a = dot_nt(x, dense_gate[...])
-    dense_b = dot_nt(x, dense_up[...])
-    gates = jnp.broadcast_to(gate_vector[...], dense_gate.shape)
-    mixing = 1.0 / (1.0 + jnp.exp(-dot_nt(x, gates)))
-    dense = (dense_a / (1.0 + jnp.exp(-dense_a)) * dense_b * mixing).astype(BF16)
-    return units, dense
-
-
-def units_kernel(rows, gate_vector, gate, up, dense_gate, dense_up, ids, shares, units, dense):
-    units[...], dense[...] = unit_values(
-        False, rows, gate_vector, gate, up, dense_gate, dense_up, ids, shares
-    )
-
-
-def branch_kernel(
-    after, rows, gate_vector, gate, up, dense_gate, dense_up, ids, shares, down, dense_down, terms
+    a, b = halves(dense_both)
+    dense = (a / (1.0 + jnp.exp(-a)) * b * mixing).astype(BF16)
+    return jnp.concatenate([units, dense], axis=1)
+
+
+def halves(x):
+    half = x.shape[1] // 2
+    return x[:, :half], x[:, half:]
+
+
+def units_kernel(
+    rows,
+    gate_vector,
+    gate,
+    up,
+    expert_down,
+    dense_down,
+    dense_front,
+    ids,
+    shares,
+    units,
+    front,
+    down,
 ):
-    units, dense = unit_values(
-        True, rows, gate_vector, gate, up, dense_gate, dense_up, ids, shares
-    )
-    terms[...] = (dot(units, down[...]) + dot(dense, dense_down[...])).astype(BF16)
-
-
-def down_kernel(units, dense, down, dense_down, terms):
-    terms[...] = dot(units[...], down[...]) + dot(dense[...], dense_down[...])
+    units[...] = unit_values(False, rows, gate_vector, (gate, up), dense_front, ids, shares)
+    width, depth = gate.shape[1], expert_down.shape[0]
+    front[:, :width] = gate[...]
+    front[:, width:] = up[...]
+    down[:depth] = expert_down[...]
+    down[depth:] = dense_down[...]
+
+
+def branch_kernel(rows, gate_vector, front, down, dense_front, ids, shares, terms):
+    units = unit_values(True, rows, gate_vector, (front,), dense_front, ids, shares)
+    terms[...] = dot(units, down[...]).astype(BF16)
+
+
+def down_kernel(units, down, terms):
+    terms[...] = dot(units[...], down[...])
+
+
+def add_kernel(near, far, terms):
+    terms[...] = (near[...] + far[...].astype(F32)).astype(BF16).reshape(terms.shape)
+
+
+def collect_kernel(terms, copies):
+    kept, width = terms.shape[1:]
+    rows = terms[...].reshape(-1, width)
+    column = lax.broadcasted_iota(jnp.int32, (kept, rows.shape[0]), 1)
+    row = lax.broadcasted_iota(jnp.int32, (kept, rows.shape[0]), 0)
+    total = dot(jnp.where(lax.rem(column, kept) == row, 1.0, 0.0).astype(BF16), rows)
+    total = total.astype(BF16)
+    for i in range(copies.shape[0]):
+        copies[i] = total
 
 
 def estimate(rows, depth, columns):
@@ -221,46 +262,69 @@
     )
 
 
-def near_units(rows, gate_vector, gate, up, dense_gate, *rest):
-    count, depth = rows.shape
-    args = (rows, gate_vector, gate, up, dense_gate, *rest)
+def near_units(rows, gate_vector, gate, up, expert_down, dense_down, *rest):
+    args = (rows, gate_vector, gate, up, expert_down, dense_down, *rest)
+    count, depth = rows.size // rows.shape[-1], expert_down.shape[0] + dense_down.shape[0]
     return pl.pallas_call(
         units_kernel,
         out_shape=[
-            pltpu.VMEM((count, gate.shape[1]), BF16),
-            pltpu.VMEM((count, dense_gate.shape[0]), BF16),
+            pltpu.VMEM((count, depth), BF16),
+            pltpu.VMEM((gate.shape[0], 2 * gate.shape[1]), BF16),
+            pltpu.VMEM((depth, expert_down.shape[1]), BF16),
         ],
         in_specs=[VMEM] * len(args),
-        out_specs=[VMEM] * 2,
+        out_specs=[VMEM] * 3,
         compiler_params=params(8),
-        cost_estimate=estimate(count, depth, 512),
+        cost_estimate=estimate(count, rows.shape[-1], 512),
         name="near_units",
     )(*map(in_vmem, args))
 
 
-def far_terms(after, rows, *weights):
+def far_terms(rows, *weights):
+    count = rows.size // rows.shape[-1]
     return pl.pallas_call(
         branch_kernel,
-        out_shape=pltpu.VMEM(rows.shape, BF16),
-        in_specs=[ANY] + [VMEM] * (1 + len(weights)),
+        out_shape=pltpu.VMEM((count, rows.shape[-1]), BF16),
+        in_specs=[VMEM] * (1 + len(weights)),
         out_specs=VMEM,
         compiler_params=params(8),
-        cost_estimate=estimate(*rows.shape, 1024),
+        cost_estimate=estimate(count, rows.shape[-1], 1024),
         name="far_terms",
-    )(*map(in_vmem, (after, rows, *weights)))
-
-
-def near_terms(units, dense, down, dense_down):
-    args = (units, dense, down, dense_down)
+    )(*map(in_vmem, (rows, *weights)))
+
+
+def near_terms(units, down):
     return pl.pallas_call(
         down_kernel,
         out_shape=pltpu.VMEM((units.shape[0], down.shape[1]), F32),
-        in_specs=[VMEM] * 4,
+        in_specs=[VMEM] * 2,
         out_specs=VMEM,
         compiler_params=params(8),
         cost_estimate=estimate(units.shape[0], 512, down.shape[1]),
         name="near_terms",
-    )(*map(in_vmem, args))
+    )(*map(in_vmem, (units, down)))
+
+
+def added(shape, near, far):
+    return pl.pallas_call(
+        add_kernel,
+        out_shape=pltpu.VMEM(shape, BF16),
+        in_specs=[VMEM] * 2,
+        out_specs=VMEM,
+        compiler_params=params(8),
+        name="added",
+    )(*map(in_vmem, (near, far)))
+
+
+def collected(count, terms):
+    return pl.pallas_call(
+        collect_kernel,
+        out_shape=pltpu.VMEM((count, *terms.shape[1:]), BF16),
+        in_specs=[VMEM],
+        out_specs=VMEM,
+        compiler_params=params(8),
+        name="collected",
+    )(in_vmem(terms))
 
 
 def last_kernel(parts, hidden, gain, shift, out):
@@ -281,17 +345,11 @@
     return pl.pallas_call(
         last_kernel,
         out_shape=jax.ShapeDtypeStruct((hidden.shape[1], gain.shape[1]), BF16),
-        grid=(1,),
-        in_specs=[
-            VMEM,
-            pl.BlockSpec((1, *hidden.shape[1:]), lambda i: (0, 0, 0)),
-            VMEM,
-            VMEM,
-        ],
-        out_specs=pl.BlockSpec((hidden.shape[1], gain.shape[1]), lambda i: (0, 0)),
+        in_specs=[VMEM] * 4,
+        out_specs=VMEM,
         compiler_params=params(4),
         name="last_norm",
-    )(parts, hidden, gain, shift)
+    )(*map(in_vmem, (parts, hidden, gain, shift)))
 
 
 def to_all(copies, axis):
@@ -324,14 +382,10 @@
     ln2_shift,
 ):
     kept = (
-        expert_gate[0],
-        expert_up[0],
         dense_gate.T,
         dense_up.T,
         expert_ids.T,
         expert_weights.T,
-        expert_down[0],
-        dense_down,
         ln1_gain[None],
         ln1_shift[None],
         ln2_gain[None],
@@ -350,19 +404,20 @@
         cache_values,
     )
     heads, tokens, *kept = attend(lax.axis_size("tp"), operands, kept)
-    unit_weights, down_weights = (gate_vector[None], *kept[:6]), kept[6:8]
-    gain_1, shift_1, gain_2, shift_2 = kept[8:]
+    dense_front, ids, shares, gain_1, shift_1, gain_2, shift_2 = kept
     plane = lax.axis_size(PLANE)
     copies = hidden_copies(plane, to_all(heads, "tp"), tokens, gain_1, shift_1)
-    rows = to_all(copies, PLANE).reshape(-1, tokens.shape[1])
+    rows = to_all(copies, PLANE)
     rows_far = lax.ppermute(rows, "ep_2", OTHER_CORE)
-    units, dense = near_units(rows, *unit_weights)
-    terms_far = far_terms(units, rows_far, *unit_weights, *down_weights)
+    tail = (dense_front, ids, shares)
+    vector = gate_vector[None]
+    units, front, down = near_units(
+        rows, vector, expert_gate[0], expert_up[0], expert_down[0], dense_down, *tail
+    )
+    terms_far = far_terms(rows_far, vector, front, down, *tail)
     terms_here = lax.ppermute(terms_far, "ep_2", OTHER_CORE)
-    terms = near_terms(units, dense, *down_weights) + terms_here.astype(F32)
-    arrived = to_all(terms.astype(BF16).reshape(plane, -1, terms.shape[1]), PLANE)
-    owned = lax.optimization_barrier(arrived.astype(F32).sum(axis=0)).astype(BF16)
-    parts = to_all(jnp.broadcast_to(owned, (lax.axis_size("tp"), *owned.shape)), "tp")
+    terms = added(copies.shape, near_terms(units, down), terms_here)
+    parts = to_all(collected(lax.axis_size("tp"), to_all(terms, PLANE)), "tp")
     return last_norm(parts, copies, gain_2, shift_2)
 
 

time: 91.3 us -> 89.2 us (0.977)
  Pallas kernels: 7.09 us -> 5.96 us
    pallas_call x2 -> x4, Pallas kernels: 2.58 us -> 2.11 us  [the longest x1 0.92 us: near_units(): pl.pallas_call(units_kernel, out_shape=[pltpu.VMEM((count, depth), BF16),...]
where the time goes in v3:
time: 89.2 us; the launch traced here: 88.9 us
  blocking collectives  76.5 us (86%)
  Pallas kernels  5.96 us (7%)
  starting transfers between devices  3.96 us (4%)
  waiting for transfers between devices  2.34 us (3%)
    all_to_all x4, blocking collectives, to_all(): return lax.all_to_all(copies, axis, split_axis=0, concat_axis=0, tiled=True)  76.5 us
    pallas_call x1, Pallas kernels, attend(): pl.pallas_call(attend_kernel, out_shape=[pltpu.VMEM((copies, tokens.shape...  2.71 us
    ppermute x1, starting transfers between devices, per_device(): terms_here = lax.ppermute(terms_far, 'ep_2', OTHER_CORE)  2.05 us
    ppermute x1, starting transfers between devices, per_device(): rows_far = lax.ppermute(rows, 'ep_2', OTHER_CORE)  1.91 us
  transfers between devices with their start and end apart: 2, of which 2 were waited for; matrix products, arithmetic and copies ran while one was open for 0% of the time, Pallas kernels for 1%

profile of v3, /device:TPU:8, one launch (start us, length us, event | category | flops | bytes accessed | tf_op | source)
XLA Modules:
  0.0 88.9 jit_solution(15687281481084580683)
XLA Ops:
  0.0 2.7 %attend.1 = (bf16[4,2,2048]{2,1,0:T(2,128)(2,1)S(1)}, bf16[2,2048]{1,0:T(2,128)(2,1)S(1)}, bf16[32,2048]{1,0:T(8,128)(2,1)S(1)}, s32[2,256]{1,0:T(2,128)S(1)}, f...) custom-call(s32[2]{0:T(128)} %lengths_hbm.1, ...), custom_call_target="tpu_custom_call" | custom-call | tf_op jit(solution)/shard_map/attend/pallas_call | solution.py:138
  2.7 9.5 %all_to_all.20.heads = bf16[4,2,2048]{2,1,0:T(2,128)(2,1)S(1)} all-to-all(bf16[4,2,2048]{2,1,0:T(2,128)(2,1)S(1)} %get-tuple-element.17), channel_id=1, replica_groups=mesh['ep_0'=8,'ep_1'=8,'ep_2'=2,'tp'=4] {'tp'}, dimensions={0} | all-to-all | bytes 65536 | tf_op jit(solution)/shard_map/all_to_all | solution.py:356
  12.3 0.0 copy-start.4
  12.3 0.2 hidden_copies.1.hidden
  12.4 0.0 copy-start
  12.4 0.0 copy-start.1
  12.5 34.5 %all_to_all.21.rows = bf16[64,2,2048]{2,1,0:T(2,128)(2,1)S(1)} all-to-all(bf16[64,2,2048]{2,1,0:T(2,128)(2,1)S(1)} %hidden_copies.1.hidden), channel_id=1, replica_groups=mesh['ep_0'=8,'ep_1'=8,'ep_2'=2,'tp'=4] {'ep_0','ep_1'}, dimensions={0} | all-to-all | bytes 1048576 | tf_op jit(solution)/shard_map/all_to_all | solution.py:356
  46.9 1.9 %collective-permute-start = (bf16[64,2,2048]{2,1,0:T(2,128)(2,1)S(1)}, bf16[64,2,2048]{2,1,0:T(2,128)(2,1)S(1)}, u32[]{:S(2)}, u32[]{:S(2)}) collective-permute-start(bf16[64,2,2048]{2,1,0:T(2,128)(2,1)S(1)} %all_to_all.21.rows), channel_id=1, source_target_pairs={{0,4},{4,0},{1,5},{5,1},{2,6},{6,2},{3,7},{7,3},{8,12},{12,8},{9,1... | collective-permute-start | bytes 1572872 | tf_op jit(solution)/shard_map/ppermute | solution.py:411
  48.9 0.0 copy-done.4
  48.9 0.0 copy-done.2
  48.9 0.0 copy-done.3
  48.9 0.0 copy-done
  48.9 0.0 copy-done.1
  48.9 0.9 %near_units.1 = (bf16[128,144]{1,0:T(8,128)(2,1)S(1)}, bf16[2048,256]{1,0:T(8,128)(2,1)S(1)}, bf16[144,2048]{1,0:T(8,128)(2,1)S(1)}) custom-call(bf16[64,2,2048]{2,1,0:T(2,128)(2,1)S(1)} %all_to_all.21.rows, bf16[1,2048]{1,0:T(2,128)(2,1)S(1)} %broadcast_in_dim.19.gate_vector, bf16[2048,128]{1,0:T(8,128)(2,1)S(1)} %bitcast.11, ...), custom_call_target="tpu_custom_call" | custom-call | flops 268435456 | bytes 4096 | tf_op jit(solution)/shard_map/near_units/pallas_call | solution.py:268
  49.9 0.9 collective-permute-done.rows
  50.7 0.8 far_terms.1
  51.6 2.0 %collective-permute-start.1 = (bf16[128,2048]{1,0:T(8,128)(2,1)S(1)}, bf16[128,2048]{1,0:T(8,128)(2,1)S(1)}, u32[]{:S(2)}, u32[]{:S(2)}) collective-permute-start(bf16[128,2048]{1,0:T(8,128)(2,1)S(1)} %far_terms.1), channel_id=1, source_target_pairs={{0,4},{4,0},{1,5},{5,1},{2,6},{6,2},{3,7},{7,3},{8,12},{12,8},{9,1... | collective-permute-start | bytes 1572872 | tf_op jit(solution)/shard_map/ppermute | solution.py:418
  53.6 0.3 near_terms.1.near
  53.9 1.5 %collective-permute-done.1.far = bf16[128,2048]{1,0:T(8,128)(2,1)S(1)} collective-permute-done((bf16[128,2048]{1,0:T(8,128)(2,1)S(1)}, bf16[128,2048]{1,0:T(8,128)(2,1)S(1)}, u32[]{:S(2)}, u32[]{:S(2)}) %collective-permute-start.1) | collective-permute-done | bytes 524320 | tf_op jit(solution)/shard_map/ppermute | solution.py:418
  55.4 0.2 added.1
  55.5 24.6 %all_to_all.22.terms = bf16[64,2,2048]{2,1,0:T(2,128)(2,1)S(1)} all-to-all(bf16[64,2,2048]{2,1,0:T(2,128)(2,1)S(1)} %added.1), channel_id=1, replica_groups=mesh['ep_0'=8,'ep_1'=8,'ep_2'=2,'tp'=4] {'ep_0','ep_1'}, dimensions={0} | all-to-all | bytes 1048576 | tf_op jit(solution)/shard_map/all_to_all | solution.py:356
  80.2 0.2 collected.1
  80.3 7.9 %all_to_all.23.parts = bf16[4,2,2048]{2,1,0:T(2,128)(2,1)S(1)} all-to-all(bf16[4,2,2048]{2,1,0:T(2,128)(2,1)S(1)} %collected.1), channel_id=1, replica_groups=mesh['ep_0'=8,'ep_1'=8,'ep_2'=2,'tp'=4] {'tp'}, dimensions={0} | all-to-all | bytes 65536 | tf_op jit(solution)/shard_map/all_to_all | solution.py:356
  88.2 0.7 last_norm.1
  (3 shorter events, 0.0 us)
Async XLA Ops:
  12.3 36.6 %copy-start.4 = (bf16[2048]{0:T(1024)(128)(2,1)S(1)}, bf16[2048]{0:T(1024)(128)(2,1)}, u32[]{:S(2)}) copy-start(bf16[2048]{0:T(1024)(128)(2,1)} %param.35) | copy-start | bytes 12292
  12.3 36.6 %copy-start.2 = (bf16[1,128,2048]{2,1,0:T(8,128)(2,1)S(1)}, bf16[1,128,2048]{2,1,0:T(8,128)(2,1)}, u32[]{:S(2)}) copy-start(bf16[1,128,2048]{2,1,0:T(8,128)(2,1)} %param.41) | copy-start | bytes 1572868
  12.3 36.6 %copy-start.3 = (bf16[16,2048]{1,0:T(8,128)(2,1)S(1)}, bf16[16,2048]{1,0:T(8,128)(2,1)}, u32[]{:S(2)}) copy-start(bf16[16,2048]{1,0:T(8,128)(2,1)} %dense_down.1) | copy-start | bytes 196612
  12.4 36.5 %copy-start = (bf16[1,2048,128]{2,1,0:T(8,128)(2,1)S(1)}, bf16[1,2048,128]{2,1,0:T(8,128)(2,1)}, u32[]{:S(2)}) copy-start(bf16[1,2048,128]{2,1,0:T(8,128)(2,1)} %param.39) | copy-start | bytes 1572868
  12.4 36.5 %copy-start.1 = (bf16[1,2048,128]{2,1,0:T(8,128)(2,1)S(1)}, bf16[1,2048,128]{2,1,0:T(8,128)(2,1)}, u32[]{:S(2)}) copy-start(bf16[1,2048,128]{2,1,0:T(8,128)(2,1)} %param.40) | copy-start | bytes 1572868
  46.9 3.8 %collective-permute-start = (bf16[64,2,2048]{2,1,0:T(2,128)(2,1)S(1)}, bf16[64,2,2048]{2,1,0:T(2,128)(2,1)S(1)}, u32[]{:S(2)}, u32[]{:S(2)}) collective-permute-start(bf16[64,2,2048]{2,1,0:T(2,128)(2,1)S(1)} %all_to_all.21.rows), channel_id=1, source_target_pairs={{0,4},{4,0},{1,5},{5,1},{2,6},{6,2},{3,7},{7,3},{8,12},{12,8},{9,1... | collective-permute-start | bytes 1572872 | tf_op jit(solution)/shard_map/ppermute | solution.py:411
  51.6 3.8 %collective-permute-start.1 = (bf16[128,2048]{1,0:T(8,128)(2,1)S(1)}, bf16[128,2048]{1,0:T(8,128)(2,1)S(1)}, u32[]{:S(2)}, u32[]{:S(2)}) collective-permute-start(bf16[128,2048]{1,0:T(8,128)(2,1)S(1)} %far_terms.1), channel_id=1, source_target_pairs={{0,4},{4,0},{1,5},{5,1},{2,6},{6,2},{3,7},{7,3},{8,12},{12,8},{9,1... | collective-permute-start | bytes 1572872 | tf_op jit(solution)/shard_map/ppermute | solution.py:418

commit v4 on v3

--- a/solution.py
+++ b/solution.py
@@ -10,7 +10,6 @@
 
 EP = ("ep_0", "ep_1", "ep_2")
 EP_TP = ("ep_0", "ep_1", "ep_2", "tp")
-PLANE = ("ep_0", "ep_1")
 OTHER_CORE = ((0, 1), (1, 0))
 
 alpha_scale = 1.4142135623730951
@@ -54,9 +53,9 @@
     *rest,
 ):
     kept = (len(rest) - 12) // 2
-    sources, (terms, tokens, *places) = rest[:kept], rest[kept : 2 * kept + 1]
-    scratch = rest[2 * kept + 1 :]
-    lengths, w_forget, cache_gates, q_v, k_v, v_v, o_v, keys_v, values_v, sems, kept_sems = scratch
+    sources, (terms, *places) = rest[:kept], rest[kept : 2 * kept]
+    scratch = rest[2 * kept :]
+    lengths, tokens, w_forget, cache_gates, q_v, k_v, v_v, o_v, keys_v, values_v, sems, kept_sems = scratch
     width = w_query.shape[1]
     moves = [
         pltpu.make_async_copy(src, dst, sems.at[i])
@@ -122,7 +121,8 @@
     new_value = dot(x, v_v[...]).astype(BF16)
     weighted = weighted + own_prob.astype(F32) * new_value.astype(F32)
     moves[9].wait()
-    term = dot(weighted.astype(BF16), o_v[...]).astype(BF16)
+    term = dot(weighted.astype(BF16), o_v[...])
+    term = (term + (alpha_scale / lax.axis_size("tp")) * x.astype(F32)).astype(BF16)
     for i in range(terms.shape[0]):
         terms[i] = term
     for move in kept_moves:
@@ -134,15 +134,14 @@
     lengths, tokens, w_forget, gates, w_query, w_key, w_value, w_output, keys, values = operands[:10]
     dense_gate, dense_up = kept[:2]
     joined = ((2 * dense_gate.shape[0], dense_gate.shape[1]),)
-    held = (w_forget, gates, w_query, w_key, w_value, w_output, keys, values)
+    held = (tokens, w_forget, gates, w_query, w_key, w_value, w_output, keys, values)
     return pl.pallas_call(
         attend_kernel,
         out_shape=[pltpu.VMEM((copies, tokens.shape[0], w_output.shape[1]), BF16)]
-        + [pltpu.VMEM(tokens.shape, BF16)]
         + [pltpu.VMEM(shape, BF16) for shape in joined]
         + [pltpu.VMEM(a.shape, a.dtype) for a in kept[2:]],
         in_specs=[pl.BlockSpec(memory_space=pltpu.HBM)] * len(operands),
-        out_specs=[VMEM] * (len(kept) + 1),
+        out_specs=[VMEM] * len(kept),
         scratch_shapes=[
             pltpu.SMEM(lengths.shape, jnp.int32),
             *(pltpu.VMEM(a.shape, a.dtype) for a in held),
@@ -160,25 +159,37 @@
     return (rows - row_mean) * lax.rsqrt(row_var + norm_eps)
 
 
-def hidden_kernel(heads, tokens, gain, shift, copies):
-    attention = heads[0].astype(F32)
-    for i in range(1, heads.shape[0]):
-        attention = attention + heads[i].astype(F32)
-    rows = alpha_scale * tokens[...].astype(F32) + attention
-    hidden = (normed(rows, rows.shape[1]) * gain[...] + shift[...]).astype(BF16)
+def picking(shape, rule):
+    row = lax.broadcasted_iota(jnp.int32, shape, 0)
+    column = lax.broadcasted_iota(jnp.int32, shape, 1)
+    return jnp.where(rule(row, column), 1.0, 0.0).astype(BF16)
+
+
+def hidden_kernel(heads, gain, shift, copies):
+    kept, width = heads.shape[1:]
+    terms = heads[...].reshape(-1, width)
+    rows = copies.shape[1]
+    spread = terms.shape[0] // rows
+    pick = picking(
+        (rows, terms.shape[0]),
+        lambda i, j: (i // kept == j // (kept * spread)) & (lax.rem(i, kept) == lax.rem(j, kept)),
+    )
+    rows = dot(pick, terms)
+    hidden = (normed(rows, width) * gain[...] + shift[...]).astype(BF16)
     for i in range(copies.shape[0]):
         copies[i] = hidden
 
 
-def hidden_copies(count, heads, tokens, gain, shift):
+def hidden_copies(side, heads, gain, shift):
+    kept, width = heads.shape[1:]
     return pl.pallas_call(
         hidden_kernel,
-        out_shape=pltpu.VMEM((count, *tokens.shape), BF16),
-        in_specs=[VMEM] * 4,
+        out_shape=pltpu.VMEM((side, side * kept, width), BF16),
+        in_specs=[VMEM] * 3,
         out_specs=VMEM,
         compiler_params=params(4),
         name="hidden_copies",
-    )(in_vmem(heads), tokens, in_vmem(gain), in_vmem(shift))
+    )(*map(in_vmem, (heads, gain, shift)))
 
 
 def unit_values(far, rows, gate_vector, front, dense_front, ids, shares):
@@ -186,7 +197,7 @@
     core = lax.axis_index("ep_2")
     expert = (lax.axis_index("ep_0") * lax.axis_size("ep_1") + lax.axis_index("ep_1")) * 2 + core
     side = 1 - core if far else core
-    x = rows[...].reshape(-1, rows.shape[2])
+    x = rows[...]
     count = x.shape[0]
     both = [dot(x, w[...]) for w in front]
     dense_both = dot_nt(x, dense_front[...])
@@ -194,7 +205,11 @@
     share_row = picked[0:1] + picked[1:2]
     row = lax.broadcasted_iota(jnp.int32, (count, tokens), 0)
     column = lax.broadcasted_iota(jnp.int32, (count, tokens), 1)
-    match = column == 4 * (row >> 1) + 2 * side + (row & 1)
+    line = lax.axis_size("ep_0")
+    outer, inner = row // (2 * line), (row // 2) % line
+    far_z = jnp.where(side == 0, inner, outer)
+    far_y = jnp.where(side == 0, outer, inner)
+    match = column == 4 * (far_z * line + far_y) + 2 * side + (row & 1)
     share = jnp.sum(jnp.where(match, share_row, 0.0), axis=1, keepdims=True)
     mixed = jnp.sum(x.astype(F32) * gate_vector[...].astype(F32), axis=1, keepdims=True)
     mixing = 1.0 / (1.0 + jnp.exp(-mixed))
@@ -242,18 +257,16 @@
 
 
 def add_kernel(near, far, terms):
-    terms[...] = (near[...] + far[...].astype(F32)).astype(BF16).reshape(terms.shape)
+    terms[...] = (near[...] + far[...].astype(F32)).astype(BF16)
 
 
 def collect_kernel(terms, copies):
-    kept, width = terms.shape[1:]
-    rows = terms[...].reshape(-1, width)
-    column = lax.broadcasted_iota(jnp.int32, (kept, rows.shape[0]), 1)
-    row = lax.broadcasted_iota(jnp.int32, (kept, rows.shape[0]), 0)
-    total = dot(jnp.where(lax.rem(column, kept) == row, 1.0, 0.0).astype(BF16), rows)
-    total = total.astype(BF16)
-    for i in range(copies.shape[0]):
-        copies[i] = total
+    total = terms[0].astype(F32)
+    for i in range(1, terms.shape[0]):
+        total = total + terms[i].astype(F32)
+    total = total.astype(BF16).reshape(copies.shape[0], *copies.shape[2:])
+    for i in range(copies.shape[1]):
+        copies[:, i] = total
 
 
 def estimate(rows, depth, columns):
@@ -305,10 +318,10 @@
     )(*map(in_vmem, (units, down)))
 
 
-def added(shape, near, far):
+def added(near, far):
     return pl.pallas_call(
         add_kernel,
-        out_shape=pltpu.VMEM(shape, BF16),
+        out_shape=pltpu.VMEM(far.shape, BF16),
         in_specs=[VMEM] * 2,
         out_specs=VMEM,
         compiler_params=params(8),
@@ -317,9 +330,10 @@
 
 
 def collected(count, terms):
+    side, rows, width = terms.shape
     return pl.pallas_call(
         collect_kernel,
-        out_shape=pltpu.VMEM((count, *terms.shape[1:]), BF16),
+        out_shape=pltpu.VMEM((side, count, rows // side, width), BF16),
         in_specs=[VMEM],
         out_specs=VMEM,
         compiler_params=params(8),
@@ -328,10 +342,13 @@
 
 
 def last_kernel(parts, hidden, gain, shift, out):
-    branches = parts[0].astype(F32)
-    for i in range(1, parts.shape[0]):
-        branches = branches + parts[i].astype(F32)
-    rows = alpha_scale * hidden[0].astype(F32) + branches
+    kept = parts.shape[1]
+    terms = parts[...].reshape(-1, parts.shape[2])
+    core = lax.axis_index("ep_2")
+    at = jnp.where(core == 0, lax.axis_index("ep_0"), lax.axis_index("ep_1"))
+    pick = picking((kept, terms.shape[0]), lambda i, j: lax.rem(j, kept) == i)
+    own = picking((kept, hidden.shape[1]), lambda i, j: j == at * kept + i)
+    rows = alpha_scale * dot(own, hidden[0]) + dot(pick, terms)
     rows = normed(rows, rows.shape[1])
     width = out.shape[1]
     place = lax.axis_index("tp")
@@ -344,7 +361,7 @@
 def last_norm(parts, hidden, gain, shift):
     return pl.pallas_call(
         last_kernel,
-        out_shape=jax.ShapeDtypeStruct((hidden.shape[1], gain.shape[1]), BF16),
+        out_shape=jax.ShapeDtypeStruct((parts.shape[1], gain.shape[1]), BF16),
         in_specs=[VMEM] * 4,
         out_specs=VMEM,
         compiler_params=params(4),
@@ -352,8 +369,25 @@
     )(*map(in_vmem, (parts, hidden, gain, shift)))
 
 
-def to_all(copies, axis):
-    return lax.all_to_all(copies, axis, split_axis=0, concat_axis=0, tiled=True)
+def lines(side, wide):
+    z, y, c = (side * 2, 2, 1)
+    alike = range(side)
+    along_y = [[z * i + y * j for j in alike] for i in alike]
+    along_z = [[z * i + y * j for i in alike] for j in alike]
+    if wide:
+        ways = range(wide)
+        groups = along_z + [[g + c for g in group] for group in along_y]
+        return [[g * wide + x for g in group for x in ways] for group in groups]
+    return along_y + [[g + c for g in group] for group in along_z]
+
+
+def along(array, side):
+    return lax.all_to_all(array, EP, 0, 0, axis_index_groups=lines(side, 0), tiled=True)
+
+
+def across(array, side, ways):
+    groups = lines(side, ways)
+    return lax.all_to_all(array, EP_TP, 0, 0, axis_index_groups=groups, tiled=True)
 
 
 def per_device(
@@ -403,11 +437,11 @@
         cache_keys,
         cache_values,
     )
-    heads, tokens, *kept = attend(lax.axis_size("tp"), operands, kept)
+    side, ways = lax.axis_size("ep_0"), lax.axis_size("tp")
+    heads, *kept = attend(side * ways, operands, kept)
     dense_front, ids, shares, gain_1, shift_1, gain_2, shift_2 = kept
-    plane = lax.axis_size(PLANE)
-    copies = hidden_copies(plane, to_all(heads, "tp"), tokens, gain_1, shift_1)
-    rows = to_all(copies, PLANE)
+    copies = hidden_copies(side, across(heads, side, ways), gain_1, shift_1)
+    rows = along(copies, side).reshape(-1, tokens.shape[1])
     rows_far = lax.ppermute(rows, "ep_2", OTHER_CORE)
     tail = (dense_front, ids, shares)
     vector = gate_vector[None]
@@ -416,8 +450,9 @@
     )
     terms_far = far_terms(rows_far, vector, front, down, *tail)
     terms_here = lax.ppermute(terms_far, "ep_2", OTHER_CORE)
-    terms = added(copies.shape, near_terms(units, down), terms_here)
-    parts = to_all(collected(lax.axis_size("tp"), to_all(terms, PLANE)), "tp")
+    terms = added(near_terms(units, down), terms_here).reshape(copies.shape)
+    sums = collected(ways, along(terms, side))
+    parts = across(sums.reshape(-1, *sums.shape[2:]), side, ways)
     return last_norm(parts, copies, gain_2, shift_2)
 
 

time: 89.2 us -> 87.5 us (0.981)
  blocking collectives: 76.5 us -> 74.7 us
    all_to_all x4, blocking collectives: 76.5 us -> 74.7 us  [the longest x2 39.7 us: across(): lax.all_to_all(array, EP_TP, 0, 0, axis_index_groups=groups, tiled=True)]
where the time goes in v4:
time: 87.5 us; the launch traced here: 87.2 us
  blocking collectives  74.7 us (85%)
  Pallas kernels  5.88 us (7%)
  starting transfers between devices  3.95 us (5%)
  waiting for transfers between devices  2.48 us (3%)
    all_to_all x2, blocking collectives, across(): lax.all_to_all(array, EP_TP, 0, 0, axis_index_groups=groups, tiled=True)  39.7 us
    all_to_all x2, blocking collectives, along(): lax.all_to_all(array, EP, 0, 0, axis_index_groups=lines(side, 0), tiled=T...  35 us
    pallas_call x1, Pallas kernels, attend(): pl.pallas_call(attend_kernel, out_shape=[pltpu.VMEM((copies, tokens.shape...  2.72 us
    ppermute x1, starting transfers between devices, per_device(): terms_here = lax.ppermute(terms_far, 'ep_2', OTHER_CORE)  2.04 us
    ppermute x1, starting transfers between devices, per_device(): rows_far = lax.ppermute(rows, 'ep_2', OTHER_CORE)  1.91 us
  transfers between devices with their start and end apart: 2, of which 2 were waited for; matrix products, arithmetic and copies ran while one was open for 0% of the time, Pallas kernels for 1%

profile of v4, /device:TPU:8, one launch (start us, length us, event | category | flops | bytes accessed | tf_op | source)
XLA Modules:
  0.0 87.2 jit_solution(13164700277241920142)
XLA Ops:
  0.0 2.7 %attend.1 = (bf16[32,2,2048]{2,1,0:T(2,128)(2,1)S(1)}, bf16[32,2048]{1,0:T(8,128)(2,1)S(1)}, s32[2,256]{1,0:T(2,128)S(1)}, f32[2,256]{1,0:T(2,128)S(1)}, f32[1,2...) custom-call(s32[2]{0:T(128)} %lengths_hbm.1, ...), custom_call_target="tpu_custom_call" | custom-call | tf_op jit(solution)/shard_map/attend/pallas_call | solution.py:138
  2.7 24.5 %all_to_all.20.heads = bf16[32,2,2048]{2,1,0:T(2,128)(2,1)S(1)} all-to-all(bf16[32,2,2048]{2,1,0:T(2,128)(2,1)S(1)} %get-tuple-element.16), channel_id=1, replica_groups={{0,1,2,3,64,65,66,67,128,129,130,131,192,193,194,195,256,257,258,259,32..., dimensions={0} | all-to-all | bytes 524288 | tf_op jit(solution)/shard_map/all_to_all | solution.py:390
  27.2 0.0 copy-start.4
  27.2 0.3 hidden_copies.1.hidden
  27.5 0.0 copy-start
  27.6 0.0 copy-start.1
  27.6 19.3 %all_to_all.21 = bf16[8,16,2048]{2,1,0:T(8,128)(2,1)S(1)} all-to-all(bf16[8,16,2048]{2,1,0:T(8,128)(2,1)S(1)} %hidden_copies.1.hidden), channel_id=1, replica_groups={{0,8,16,24,32,40,48,56},{64,72,80,88,96,104,112,120},{128,136,144,152,1..., dimensions={0} | all-to-all | bytes 1048576 | tf_op jit(solution)/shard_map/all_to_all | solution.py:385
  46.9 1.9 %collective-permute-start = (bf16[128,2048]{1,0:T(8,128)(2,1)S(1)}, bf16[128,2048]{1,0:T(8,128)(2,1)S(1)}, u32[]{:S(2)}, u32[]{:S(2)}) collective-permute-start(bf16[128,2048]{1,0:T(8,128)(2,1)S(1)} %bitcast.14), channel_id=1, source_target_pairs={{0,4},{4,0},{1,5},{5,1},{2,6},{6,2},{3,7},{7,3},{8,12},{12,8},{9,1... | collective-permute-start | bytes 1572872 | tf_op jit(solution)/shard_map/ppermute | solution.py:445
  48.8 0.0 copy-done.4
  48.8 0.0 copy-done.2
  48.8 0.0 copy-done.3
  48.8 0.0 copy-done
  48.9 0.0 copy-done.1
  48.9 0.8 near_units.1
  49.7 1.0 %collective-permute-done.rows = bf16[128,2048]{1,0:T(8,128)(2,1)S(1)} collective-permute-done((bf16[128,2048]{1,0:T(8,128)(2,1)S(1)}, bf16[128,2048]{1,0:T(8,128)(2,1)S(1)}, u32[]{:S(2)}, u32[]{:S(2)}) %collective-permute-start) | collective-permute-done | bytes 524320 | tf_op jit(solution)/shard_map/ppermute | solution.py:445
  50.7 0.8 far_terms.1
  51.4 2.0 %collective-permute-start.1 = (bf16[128,2048]{1,0:T(8,128)(2,1)S(1)}, bf16[128,2048]{1,0:T(8,128)(2,1)S(1)}, u32[]{:S(2)}, u32[]{:S(2)}) collective-permute-start(bf16[128,2048]{1,0:T(8,128)(2,1)S(1)} %far_terms.1), channel_id=1, source_target_pairs={{0,4},{4,0},{1,5},{5,1},{2,6},{6,2},{3,7},{7,3},{8,12},{12,8},{9,1... | collective-permute-start | bytes 1572872 | tf_op jit(solution)/shard_map/ppermute | solution.py:452
  53.5 0.3 near_terms.1.near
  53.8 1.5 %collective-permute-done.1.far = bf16[128,2048]{1,0:T(8,128)(2,1)S(1)} collective-permute-done((bf16[128,2048]{1,0:T(8,128)(2,1)S(1)}, bf16[128,2048]{1,0:T(8,128)(2,1)S(1)}, u32[]{:S(2)}, u32[]{:S(2)}) %collective-permute-start.1) | collective-permute-done | bytes 524320 | tf_op jit(solution)/shard_map/ppermute | solution.py:452
  55.2 0.1 added.1
  55.3 15.7 %all_to_all.22.terms = bf16[8,16,2048]{2,1,0:T(8,128)(2,1)S(1)} all-to-all(bf16[8,16,2048]{2,1,0:T(8,128)(2,1)S(1)} %bitcast.16), channel_id=1, replica_groups={{0,8,16,24,32,40,48,56},{64,72,80,88,96,104,112,120},{128,136,144,152,1..., dimensions={0} | all-to-all | bytes 1048576 | tf_op jit(solution)/shard_map/all_to_all | solution.py:385
  71.0 0.1 collected.1
  71.1 15.2 %all_to_all.23.parts = bf16[32,2,2048]{2,1,0:T(2,128)(2,1)S(1)} all-to-all(bf16[32,2,2048]{2,1,0:T(2,128)(2,1)S(1)} %bitcast.17), channel_id=1, replica_groups={{0,1,2,3,64,65,66,67,128,129,130,131,192,193,194,195,256,257,258,259,32..., dimensions={0} | all-to-all | bytes 524288 | tf_op jit(solution)/shard_map/all_to_all | solution.py:390
  86.3 0.9 last_norm.1
  (3 shorter events, 0.0 us)
Async XLA Ops:
  27.2 21.6 %copy-start.4 = (bf16[2048]{0:T(1024)(128)(2,1)S(1)}, bf16[2048]{0:T(1024)(128)(2,1)}, u32[]{:S(2)}) copy-start(bf16[2048]{0:T(1024)(128)(2,1)} %param.35) | copy-start | bytes 12292
  27.2 21.6 %copy-start.2 = (bf16[1,128,2048]{2,1,0:T(8,128)(2,1)S(1)}, bf16[1,128,2048]{2,1,0:T(8,128)(2,1)}, u32[]{:S(2)}) copy-start(bf16[1,128,2048]{2,1,0:T(8,128)(2,1)} %param.41) | copy-start | bytes 1572868
  27.2 21.6 %copy-start.3 = (bf16[16,2048]{1,0:T(8,128)(2,1)S(1)}, bf16[16,2048]{1,0:T(8,128)(2,1)}, u32[]{:S(2)}) copy-start(bf16[16,2048]{1,0:T(8,128)(2,1)} %dense_down.1) | copy-start | bytes 196612
  27.5 21.3 %copy-start = (bf16[1,2048,128]{2,1,0:T(8,128)(2,1)S(1)}, bf16[1,2048,128]{2,1,0:T(8,128)(2,1)}, u32[]{:S(2)}) copy-start(bf16[1,2048,128]{2,1,0:T(8,128)(2,1)} %param.39) | copy-start | bytes 1572868
  27.6 21.3 %copy-start.1 = (bf16[1,2048,128]{2,1,0:T(8,128)(2,1)S(1)}, bf16[1,2048,128]{2,1,0:T(8,128)(2,1)}, u32[]{:S(2)}) copy-start(bf16[1,2048,128]{2,1,0:T(8,128)(2,1)} %param.40) | copy-start | bytes 1572868
  46.9 3.8 %collective-permute-start = (bf16[128,2048]{1,0:T(8,128)(2,1)S(1)}, bf16[128,2048]{1,0:T(8,128)(2,1)S(1)}, u32[]{:S(2)}, u32[]{:S(2)}) collective-permute-start(bf16[128,2048]{1,0:T(8,128)(2,1)S(1)} %bitcast.14), channel_id=1, source_target_pairs={{0,4},{4,0},{1,5},{5,1},{2,6},{6,2},{3,7},{7,3},{8,12},{12,8},{9,1... | collective-permute-start | bytes 1572872 | tf_op jit(solution)/shard_map/ppermute | solution.py:445
  51.4 3.8 %collective-permute-start.1 = (bf16[128,2048]{1,0:T(8,128)(2,1)S(1)}, bf16[128,2048]{1,0:T(8,128)(2,1)S(1)}, u32[]{:S(2)}, u32[]{:S(2)}) collective-permute-start(bf16[128,2048]{1,0:T(8,128)(2,1)S(1)} %far_terms.1), channel_id=1, source_target_pairs={{0,4},{4,0},{1,5},{5,1},{2,6},{6,2},{3,7},{7,3},{8,12},{12,8},{9,1... | collective-permute-start | bytes 1572872 | tf_op jit(solution)/shard_map/ppermute | solution.py:452

commit v5 on v4

--- a/solution.py
+++ b/solution.py
@@ -12,6 +12,8 @@
 EP_TP = ("ep_0", "ep_1", "ep_2", "tp")
 OTHER_CORE = ((0, 1), (1, 0))
 
+EXPERT_UNITS = 128
+DENSE_UNITS = 16
 alpha_scale = 1.4142135623730951
 norm_eps = 1e-05
 
@@ -52,9 +54,9 @@
     cache_values,
     *rest,
 ):
-    kept = (len(rest) - 12) // 2
-    sources, (terms, *places) = rest[:kept], rest[kept : 2 * kept]
-    scratch = rest[2 * kept :]
+    kept = (len(rest) - 8) // 2
+    sources, (terms, *places) = rest[:kept], rest[kept : 2 * kept - 4]
+    scratch = rest[2 * kept - 4 :]
     lengths, tokens, w_forget, cache_gates, q_v, k_v, v_v, o_v, keys_v, values_v, sems, kept_sems = scratch
     width = w_query.shape[1]
     moves = [
@@ -75,12 +77,24 @@
         )
     ]
     targets = list(places)
-    dense_front = places[0]
-    rows = dense_front.shape[0] // 2
-    targets[:1] = (dense_front.at[:rows], dense_front.at[rows:])
+    pool = places[0]
+    gate, up, down, *dense = sources[:6]
+    depth, width_up = pool.shape[1], gate.shape[1]
+    rows = gate.shape[0] * 2 * width_up // depth
+    pieces = []
+    for k in range(gate.shape[0] // rows):
+        for n, source in enumerate((gate, up)):
+            start = (2 * k + n) * width_up
+            pieces.append(
+                (source.at[rows * k : rows * (k + 1)], pool.at[:rows, start : start + width_up])
+            )
+    for source in (down, *dense):
+        pieces.append((source, pool.at[rows : rows + source.shape[0]]))
+        rows += source.shape[0]
+    pieces += zip(sources[6:], places[1:])
     kept_moves = [
         pltpu.make_async_copy(src, dst, kept_sems.at[i])
-        for i, (src, dst) in enumerate(zip(sources, targets))
+        for i, (src, dst) in enumerate(pieces)
     ]
     for move in moves + kept_moves:
         move.start()
@@ -129,24 +143,29 @@
         move.wait()
 
 
+def rows_of(gate, line):
+    return 2 * gate.size // line
+
+
 def attend(copies, operands, kept):
     operands = [pltpu.with_memory_space_constraint(a, pltpu.HBM) for a in (*operands, *kept)]
     lengths, tokens, w_forget, gates, w_query, w_key, w_value, w_output, keys, values = operands[:10]
-    dense_gate, dense_up = kept[:2]
-    joined = ((2 * dense_gate.shape[0], dense_gate.shape[1]),)
+    gate, up, down, *dense = kept[:6]
+    line = down.shape[1]
+    rows = (gate.size + up.size) // line + down.shape[0] + sum(a.shape[0] for a in dense)
     held = (tokens, w_forget, gates, w_query, w_key, w_value, w_output, keys, values)
     return pl.pallas_call(
         attend_kernel,
         out_shape=[pltpu.VMEM((copies, tokens.shape[0], w_output.shape[1]), BF16)]
-        + [pltpu.VMEM(shape, BF16) for shape in joined]
-        + [pltpu.VMEM(a.shape, a.dtype) for a in kept[2:]],
+        + [pltpu.VMEM((rows, line), BF16)]
+        + [pltpu.VMEM(a.shape, a.dtype) for a in kept[6:]],
         in_specs=[pl.BlockSpec(memory_space=pltpu.HBM)] * len(operands),
-        out_specs=[VMEM] * len(kept),
+        out_specs=[VMEM] * (len(kept) - 4),
         scratch_shapes=[
             pltpu.SMEM(lengths.shape, jnp.int32),
             *(pltpu.VMEM(a.shape, a.dtype) for a in held),
             pltpu.SemaphoreType.DMA((10,)),
-            pltpu.SemaphoreType.DMA((len(kept),)),
+            pltpu.SemaphoreType.DMA((len(kept) + 2 * gate.size // (rows_of(gate, line) * gate.shape[1]),)),
         ],
         compiler_params=params(12),
         name="attend",
@@ -192,72 +211,51 @@
     )(*map(in_vmem, (heads, gain, shift)))
 
 
-def unit_values(far, rows, gate_vector, front, dense_front, ids, shares):
-    tokens = ids.shape[1]
-    core = lax.axis_index("ep_2")
-    expert = (lax.axis_index("ep_0") * lax.axis_size("ep_1") + lax.axis_index("ep_1")) * 2 + core
-    side = 1 - core if far else core
-    x = rows[...]
-    count = x.shape[0]
-    both = [dot(x, w[...]) for w in front]
-    dense_both = dot_nt(x, dense_front[...])
-    picked = jnp.where(ids[...] == expert, shares[...], 0.0)
-    share_row = picked[0:1] + picked[1:2]
-    row = lax.broadcasted_iota(jnp.int32, (count, tokens), 0)
-    column = lax.broadcasted_iota(jnp.int32, (count, tokens), 1)
-    line = lax.axis_size("ep_0")
-    outer, inner = row // (2 * line), (row // 2) % line
-    far_z = jnp.where(side == 0, inner, outer)
-    far_y = jnp.where(side == 0, outer, inner)
-    match = column == 4 * (far_z * line + far_y) + 2 * side + (row & 1)
-    share = jnp.sum(jnp.where(match, share_row, 0.0), axis=1, keepdims=True)
-    mixed = jnp.sum(x.astype(F32) * gate_vector[...].astype(F32), axis=1, keepdims=True)
-    mixing = 1.0 / (1.0 + jnp.exp(-mixed))
-    a, b = halves(both[0]) if len(both) == 1 else both
-    units = (a / (1.0 + jnp.exp(-a)) * b * share).astype(BF16)
-    a, b = halves(dense_both)
-    dense = (a / (1.0 + jnp.exp(-a)) * b * mixing).astype(BF16)
-    return jnp.concatenate([units, dense], axis=1)
-
-
 def halves(x):
     half = x.shape[1] // 2
     return x[:, :half], x[:, half:]
 
 
-def units_kernel(
-    rows,
-    gate_vector,
-    gate,
-    up,
-    expert_down,
-    dense_down,
-    dense_front,
-    ids,
-    shares,
-    units,
-    front,
-    down,
-):
-    units[...] = unit_values(False, rows, gate_vector, (gate, up), dense_front, ids, shares)
-    width, depth = gate.shape[1], expert_down.shape[0]
-    front[:, :width] = gate[...]
-    front[:, width:] = up[...]
-    down[:depth] = expert_down[...]
-    down[depth:] = dense_down[...]
-
-
-def branch_kernel(rows, gate_vector, front, down, dense_front, ids, shares, terms):
-    units = unit_values(True, rows, gate_vector, (front,), dense_front, ids, shares)
-    terms[...] = dot(units, down[...]).astype(BF16)
-
-
-def down_kernel(units, down, terms):
-    terms[...] = dot(units[...], down[...])
-
-
-def add_kernel(near, far, terms):
-    terms[...] = (near[...] + far[...].astype(F32)).astype(BF16)
+def branch_kernel(rows, gate_vector, mine, other, ids, shares, terms):
+    x = rows[...]
+    count, depth = x.shape
+    tokens, line = ids.shape[1], lax.axis_size("ep_0")
+    core = lax.axis_index("ep_2")
+    chip = lax.axis_index("ep_0") * line + lax.axis_index("ep_1")
+    row = lax.broadcasted_iota(jnp.int32, (count, tokens), 0)
+    column = lax.broadcasted_iota(jnp.int32, (count, tokens), 1)
+    outer, inner = row // (2 * line), (row // 2) % line
+    far_z = jnp.where(core == 0, inner, outer)
+    far_y = jnp.where(core == 0, outer, inner)
+    match = column == 4 * (far_z * line + far_y) + 2 * core + (row & 1)
+    lanes = gate_vector.shape[1]
+    mixed = jnp.zeros((count, lanes), F32)
+    for k in range(gate_vector.shape[0]):
+        part = x[:, k * lanes : (k + 1) * lanes].astype(F32)
+        mixed = mixed + part * gate_vector[k : k + 1].astype(F32)
+    mixed = jnp.sum(mixed, axis=1, keepdims=True)
+    mixing = 1.0 / (1.0 + jnp.exp(-mixed))
+    split = 2 * EXPERT_UNITS
+    units = []
+    for pool, expert in ((mine, chip * 2 + core), (other, chip * 2 + 1 - core)):
+        both = dot(x[:, :split], pool[:split, :split])
+        for k in range(split, depth, split):
+            both = both + dot(x[:, k : k + split], pool[:split, k : k + split])
+        dense_both = dot_nt(x, pool[split + EXPERT_UNITS + DENSE_UNITS :])
+        picked = jnp.where(ids[...] == expert, shares[...], 0.0)
+        share_row = picked[0:1] + picked[1:2]
+        share = jnp.sum(jnp.where(match, share_row, 0.0), axis=1, keepdims=True)
+        a, b = halves(both)
+        wide = (a / (1.0 + jnp.exp(-a)) * b * share).astype(BF16)
+        a, b = halves(dense_both)
+        narrow = (a / (1.0 + jnp.exp(-a)) * b * mixing).astype(BF16)
+        units.append(jnp.concatenate([wide, narrow], axis=1))
+    end = split + EXPERT_UNITS + DENSE_UNITS
+    step = 512
+    for k in range(0, depth, step):
+        total = dot(units[0], mine[split:end, k : k + step])
+        total = total + dot(units[1], other[split:end, k : k + step])
+        terms[:, k : k + step] = total.astype(BF16)
 
 
 def collect_kernel(terms, copies):
@@ -269,64 +267,19 @@
         copies[:, i] = total
 
 
-def estimate(rows, depth, columns):
-    return pl.CostEstimate(
-        flops=2 * rows * depth * columns, bytes_accessed=4096, transcendentals=0
-    )
-
-
-def near_units(rows, gate_vector, gate, up, expert_down, dense_down, *rest):
-    args = (rows, gate_vector, gate, up, expert_down, dense_down, *rest)
-    count, depth = rows.size // rows.shape[-1], expert_down.shape[0] + dense_down.shape[0]
-    return pl.pallas_call(
-        units_kernel,
-        out_shape=[
-            pltpu.VMEM((count, depth), BF16),
-            pltpu.VMEM((gate.shape[0], 2 * gate.shape[1]), BF16),
-            pltpu.VMEM((depth, expert_down.shape[1]), BF16),
-        ],
-        in_specs=[VMEM] * len(args),
-        out_specs=[VMEM] * 3,
-        compiler_params=params(8),
-        cost_estimate=estimate(count, rows.shape[-1], 512),
-        name="near_units",
-    )(*map(in_vmem, args))
-
-
-def far_terms(rows, *weights):
-    count = rows.size // rows.shape[-1]
+def branch_terms(*args):
+    rows = args[0]
     return pl.pallas_call(
         branch_kernel,
-        out_shape=pltpu.VMEM((count, rows.shape[-1]), BF16),
-        in_specs=[VMEM] * (1 + len(weights)),
+        out_shape=pltpu.VMEM(rows.shape, BF16),
+        in_specs=[VMEM] * len(args),
         out_specs=VMEM,
         compiler_params=params(8),
-        cost_estimate=estimate(count, rows.shape[-1], 1024),
-        name="far_terms",
-    )(*map(in_vmem, (rows, *weights)))
-
-
-def near_terms(units, down):
-    return pl.pallas_call(
-        down_kernel,
-        out_shape=pltpu.VMEM((units.shape[0], down.shape[1]), F32),
-        in_specs=[VMEM] * 2,
-        out_specs=VMEM,
-        compiler_params=params(8),
-        cost_estimate=estimate(units.shape[0], 512, down.shape[1]),
-        name="near_terms",
-    )(*map(in_vmem, (units, down)))
-
-
-def added(near, far):
-    return pl.pallas_call(
-        add_kernel,
-        out_shape=pltpu.VMEM(far.shape, BF16),
-        in_specs=[VMEM] * 2,
-        out_specs=VMEM,
-        compiler_params=params(8),
-        name="added",
-    )(*map(in_vmem, (near, far)))
+        cost_estimate=pl.CostEstimate(
+            flops=2 * rows.size * 1024, bytes_accessed=4096, transcendentals=0
+        ),
+        name="branch_terms",
+    )(*map(in_vmem, args))
 
 
 def collected(count, terms):
@@ -416,8 +369,13 @@
     ln2_shift,
 ):
     kept = (
+        expert_gate[0],
+        expert_up[0],
+        expert_down[0],
+        dense_down,
         dense_gate.T,
         dense_up.T,
+        gate_vector.reshape(-1, 128),
         expert_ids.T,
         expert_weights.T,
         ln1_gain[None],
@@ -439,18 +397,11 @@
     )
     side, ways = lax.axis_size("ep_0"), lax.axis_size("tp")
     heads, *kept = attend(side * ways, operands, kept)
-    dense_front, ids, shares, gain_1, shift_1, gain_2, shift_2 = kept
+    pool, vector, ids, shares, gain_1, shift_1, gain_2, shift_2 = kept
+    other = lax.ppermute(pool, "ep_2", OTHER_CORE)
     copies = hidden_copies(side, across(heads, side, ways), gain_1, shift_1)
     rows = along(copies, side).reshape(-1, tokens.shape[1])
-    rows_far = lax.ppermute(rows, "ep_2", OTHER_CORE)
-    tail = (dense_front, ids, shares)
-    vector = gate_vector[None]
-    units, front, down = near_units(
-        rows, vector, expert_gate[0], expert_up[0], expert_down[0], dense_down, *tail
-    )
-    terms_far = far_terms(rows_far, vector, front, down, *tail)
-    terms_here = lax.ppermute(terms_far, "ep_2", OTHER_CORE)
-    terms = added(near_terms(units, down), terms_here).reshape(copies.shape)
+    terms = branch_terms(rows, vector, pool, other, ids, shares).reshape(copies.shape)
     sums = collected(ways, along(terms, side))
     parts = across(sums.reshape(-1, *sums.shape[2:]), side, ways)
     return last_norm(parts, copies, gain_2, shift_2)

time: 87.5 us -> 82.8 us (0.946)
  waiting for transfers between devices: 2.48 us -> 0.01 us
  starting transfers between devices: 3.95 us -> 1.92 us
    ppermute x2 -> x1, waiting for transfers between devices: 2.48 us -> 0.01 us  [per_device(): other = lax.ppermute(pool, 'ep_2', OTHER_CORE)]
    ppermute x2 -> x1, starting transfers between devices: 3.95 us -> 1.92 us  [per_device(): other = lax.ppermute(pool, 'ep_2', OTHER_CORE)]
    pallas_call x4 -> x1, Pallas kernels: 1.92 us -> 1.25 us  [branch_terms(): pl.pallas_call(branch_kernel, out_shape=pltpu.VMEM(rows.shape, BF16), in_...]
  transfers between devices with their start and end apart: 2 -> 1, of which waited for: 2 -> 0; matrix products, arithmetic and copies ran while one was open for 0% -> 0% of each run, Pallas kernels for 1% -> 0%
where the time goes in v5:
time: 82.8 us; the launch traced here: 82.5 us
  blocking collectives  74.6 us (90%)
  Pallas kernels  5.96 us (7%)
  starting transfers between devices  1.92 us (2%)
    all_to_all x2, blocking collectives, across(): lax.all_to_all(array, EP_TP, 0, 0, axis_index_groups=groups, tiled=True)  39.7 us
    all_to_all x2, blocking collectives, along(): lax.all_to_all(array, EP, 0, 0, axis_index_groups=lines(side, 0), tiled=T...  34.9 us
    pallas_call x1, Pallas kernels, attend(): pl.pallas_call(attend_kernel, out_shape=[pltpu.VMEM((copies, tokens.shape...  3.48 us
    ppermute x1, starting transfers between devices, per_device(): other = lax.ppermute(pool, 'ep_2', OTHER_CORE)  1.92 us
  transfers between devices with their start and end apart: 1, of which 0 were waited for; matrix products, arithmetic and copies ran while one was open for 0% of the time, Pallas kernels for 0%

profile of v5, /device:TPU:8, one launch (start us, length us, event | category | flops | bytes accessed | tf_op | source)
XLA Modules:
  0.0 82.5 jit_solution(12566440213239150030)
XLA Ops:
  0.0 3.5 %attend.1 = (bf16[32,2,2048]{2,1,0:T(2,128)(2,1)S(1)}, bf16[432,2048]{1,0:T(8,128)(2,1)S(1)}, bf16[16,128]{1,0:T(8,128)(2,1)S(1)}, s32[2,256]{1,0:T(2,128)S(1)},...) custom-call(s32[2]{0:T(128)} %lengths_hbm.1, ...), custom_call_target="tpu_custom_call" | custom-call | tf_op jit(solution)/shard_map/attend/pallas_call | solution.py:157
  3.5 1.9 %collective-permute-start = (bf16[432,2048]{1,0:T(8,128)(2,1)S(1)}, bf16[432,2048]{1,0:T(8,128)(2,1)S(1)}, u32[]{:S(2)}, u32[]{:S(2)}) collective-permute-start(bf16[432,2048]{1,0:T(8,128)(2,1)S(1)} %get-tuple-element.18.mine), channel_id=1, source_target_pairs={{0,4},{4,0},{1,5},{5,1},{2,6},{6,2},{3,7},{7,3},{8,12},{12,8},{9,1... | collective-permute-start | bytes 5308424 | tf_op jit(solution)/shard_map/ppermute | solution.py:401
  5.4 24.5 %all_to_all.20.heads = bf16[32,2,2048]{2,1,0:T(2,128)(2,1)S(1)} all-to-all(bf16[32,2,2048]{2,1,0:T(2,128)(2,1)S(1)} %get-tuple-element.14), channel_id=1, replica_groups={{0,1,2,3,64,65,66,67,128,129,130,131,192,193,194,195,256,257,258,259,32..., dimensions={0} | all-to-all | bytes 524288 | tf_op jit(solution)/shard_map/all_to_all | solution.py:343
  29.9 0.3 hidden_copies.1.hidden
  30.2 19.2 %all_to_all.21 = bf16[8,16,2048]{2,1,0:T(8,128)(2,1)S(1)} all-to-all(bf16[8,16,2048]{2,1,0:T(8,128)(2,1)S(1)} %hidden_copies.1.hidden), channel_id=1, replica_groups={{0,8,16,24,32,40,48,56},{64,72,80,88,96,104,112,120},{128,136,144,152,1..., dimensions={0} | all-to-all | bytes 1048576 | tf_op jit(solution)/shard_map/all_to_all | solution.py:338
  49.4 0.0 collective-permute-done.other
  49.4 1.2 %branch_terms.1 = bf16[128,2048]{1,0:T(8,128)(2,1)S(1)} custom-call(bf16[128,2048]{1,0:T(8,128)(2,1)S(1)} %bitcast.15, bf16[16,128]{1,0:T(8,128)(2,1)S(1)} %get-tuple-element.17.gate_vector, bf16[432,2048]{1,0:T(8,128)(2,1)S(1)} %get-tuple-element.18.mine, bf16[432,2048]{1,0:T(8,128)(2,1)S(1)} %collective-permute-done.other, ...), custom_call_target="tpu_custom_call" | custom-call | flops 536870912 | bytes 4096 | tf_op jit(solution)/shard_map/branch_terms/pallas_call | solution.py:272
  50.7 15.7 %all_to_all.22.terms = bf16[8,16,2048]{2,1,0:T(8,128)(2,1)S(1)} all-to-all(bf16[8,16,2048]{2,1,0:T(8,128)(2,1)S(1)} %bitcast.16), channel_id=1, replica_groups={{0,8,16,24,32,40,48,56},{64,72,80,88,96,104,112,120},{128,136,144,152,1..., dimensions={0} | all-to-all | bytes 1048576 | tf_op jit(solution)/shard_map/all_to_all | solution.py:338
  66.4 0.1 collected.1
  66.5 15.2 %all_to_all.23.parts = bf16[32,2,2048]{2,1,0:T(2,128)(2,1)S(1)} all-to-all(bf16[32,2,2048]{2,1,0:T(2,128)(2,1)S(1)} %bitcast.17), channel_id=1, replica_groups={{0,1,2,3,64,65,66,67,128,129,130,131,192,193,194,195,256,257,258,259,32..., dimensions={0} | all-to-all | bytes 524288 | tf_op jit(solution)/shard_map/all_to_all | solution.py:343
  81.6 0.9 %last_norm.1 = bf16[2,512]{1,0:T(2,128)(2,1)} custom-call(bf16[32,2,2048]{2,1,0:T(2,128)(2,1)S(1)} %all_to_all.23.parts, bf16[8,16,2048]{2,1,0:T(8,128)(2,1)S(1)} %hidden_copies.1.hidden, f32[1,512]{1,0:T(1,128)S(1)} %get-tuple-element.21.gain, f32[1,512]{1,0:T(1,128)S(1)} %get-tuple-element.22.shift), custom_call_target="tpu_custom_call" | custom-call | tf_op jit(solution)/shard_map/last_norm/pallas_call | solution.py:315
Async XLA Ops:
  3.5 45.9 %collective-permute-start = (bf16[432,2048]{1,0:T(8,128)(2,1)S(1)}, bf16[432,2048]{1,0:T(8,128)(2,1)S(1)}, u32[]{:S(2)}, u32[]{:S(2)}) collective-permute-start(bf16[432,2048]{1,0:T(8,128)(2,1)S(1)} %get-tuple-element.18.mine), channel_id=1, source_target_pairs={{0,4},{4,0},{1,5},{5,1},{2,6},{6,2},{3,7},{7,3},{8,12},{12,8},{9,1... | collective-permute-start | bytes 5308424 | tf_op jit(solution)/shard_map/ppermute | solution.py:401

commit v6 on v5

--- a/solution.py
+++ b/solution.py
@@ -70,8 +70,8 @@
                 (w_query, q_v),
                 (cache_keys, keys_v),
                 (w_key, k_v),
+                (w_value, v_v),
                 (cache_values, values_v),
-                (w_value, v_v),
                 (w_output, o_v),
             )
         )
@@ -96,7 +96,7 @@
         pltpu.make_async_copy(src, dst, kept_sems.at[i])
         for i, (src, dst) in enumerate(pieces)
     ]
-    for move in moves + kept_moves:
+    for move in moves:
         move.start()
 
     for move in moves[:4]:
@@ -114,12 +114,16 @@
     decay_bias = (last_gate + forget_new) - gates
 
     moves[4].wait()
+    for move in kept_moves:
+        move.start()
     query = dot(x, q_v[...]).astype(BF16)
     moves[5].wait()
     scores = jnp.where(second, dot_nt(query, keys_v[1, 0]), dot_nt(query, keys_v[0, 0])) * scale
     scores = jnp.where(positions < used, scores + decay_bias, -jnp.inf)
     moves[6].wait()
+    moves[7].wait()
     new_key = dot(x, k_v[...]).astype(BF16)
+    new_value = dot(x, v_v[...]).astype(BF16)
     own_score = (
         jnp.sum(query.astype(F32) * new_key.astype(F32), axis=1, keepdims=True) * scale
     )
@@ -129,10 +133,8 @@
     denominator = jnp.sum(exp_terms, axis=1, keepdims=True) + own_exp
     probs = (exp_terms / denominator).astype(BF16)
     own_prob = (own_exp / denominator).astype(BF16)
-    moves[7].wait()
+    moves[8].wait()
     weighted = jnp.where(second, dot(probs, values_v[1, 0]), dot(probs, values_v[0, 0]))
-    moves[8].wait()
-    new_value = dot(x, v_v[...]).astype(BF16)
     weighted = weighted + own_prob.astype(F32) * new_value.astype(F32)
     moves[9].wait()
     term = dot(weighted.astype(BF16), o_v[...])

time: 82.8 us -> 82.4 us (level)
  no operation moved by 1% of the time
where the time goes in v6:
time: 82.4 us; the launch traced here: 82 us
  blocking collectives  74.6 us (91%)
  Pallas kernels  5.49 us (7%)
  starting transfers between devices  1.92 us (2%)
    all_to_all x2, blocking collectives, across(): lax.all_to_all(array, EP_TP, 0, 0, axis_index_groups=groups, tiled=True)  39.7 us
    all_to_all x2, blocking collectives, along(): lax.all_to_all(array, EP, 0, 0, axis_index_groups=lines(side, 0), tiled=T...  34.9 us
    pallas_call x1, Pallas kernels, attend(): pl.pallas_call(attend_kernel, out_shape=[pltpu.VMEM((copies, tokens.shape...  3 us
    ppermute x1, starting transfers between devices, per_device(): other = lax.ppermute(pool, 'ep_2', OTHER_CORE)  1.92 us
  transfers between devices with their start and end apart: 1, of which 0 were waited for; matrix products, arithmetic and copies ran while one was open for 0% of the time, Pallas kernels for 0%

profile of v6, /device:TPU:8, one launch (start us, length us, event | category | flops | bytes accessed | tf_op | source)
XLA Modules:
  0.0 82.0 jit_solution(16757752541135957545)
XLA Ops:
  0.0 3.0 %attend.1 = (bf16[32,2,2048]{2,1,0:T(2,128)(2,1)S(1)}, bf16[432,2048]{1,0:T(8,128)(2,1)S(1)}, bf16[16,128]{1,0:T(8,128)(2,1)S(1)}, s32[2,256]{1,0:T(2,128)S(1)},...) custom-call(s32[2]{0:T(128)} %lengths_hbm.1, ...), custom_call_target="tpu_custom_call" | custom-call | tf_op jit(solution)/shard_map/attend/pallas_call | solution.py:159
  3.0 1.9 %collective-permute-start = (bf16[432,2048]{1,0:T(8,128)(2,1)S(1)}, bf16[432,2048]{1,0:T(8,128)(2,1)S(1)}, u32[]{:S(2)}, u32[]{:S(2)}) collective-permute-start(bf16[432,2048]{1,0:T(8,128)(2,1)S(1)} %get-tuple-element.18.mine), channel_id=1, source_target_pairs={{0,4},{4,0},{1,5},{5,1},{2,6},{6,2},{3,7},{7,3},{8,12},{12,8},{9,1... | collective-permute-start | bytes 5308424 | tf_op jit(solution)/shard_map/ppermute | solution.py:403
  4.9 24.5 %all_to_all.20.heads = bf16[32,2,2048]{2,1,0:T(2,128)(2,1)S(1)} all-to-all(bf16[32,2,2048]{2,1,0:T(2,128)(2,1)S(1)} %get-tuple-element.14), channel_id=1, replica_groups={{0,1,2,3,64,65,66,67,128,129,130,131,192,193,194,195,256,257,258,259,32..., dimensions={0} | all-to-all | bytes 524288 | tf_op jit(solution)/shard_map/all_to_all | solution.py:345
  29.4 0.3 hidden_copies.1.hidden
  29.7 19.2 %all_to_all.21 = bf16[8,16,2048]{2,1,0:T(8,128)(2,1)S(1)} all-to-all(bf16[8,16,2048]{2,1,0:T(8,128)(2,1)S(1)} %hidden_copies.1.hidden), channel_id=1, replica_groups={{0,8,16,24,32,40,48,56},{64,72,80,88,96,104,112,120},{128,136,144,152,1..., dimensions={0} | all-to-all | bytes 1048576 | tf_op jit(solution)/shard_map/all_to_all | solution.py:340
  48.9 0.0 collective-permute-done.other
  48.9 1.3 %branch_terms.1 = bf16[128,2048]{1,0:T(8,128)(2,1)S(1)} custom-call(bf16[128,2048]{1,0:T(8,128)(2,1)S(1)} %bitcast.15, bf16[16,128]{1,0:T(8,128)(2,1)S(1)} %get-tuple-element.17.gate_vector, bf16[432,2048]{1,0:T(8,128)(2,1)S(1)} %get-tuple-element.18.mine, bf16[432,2048]{1,0:T(8,128)(2,1)S(1)} %collective-permute-done.other, ...), custom_call_target="tpu_custom_call" | custom-call | flops 536870912 | bytes 4096 | tf_op jit(solution)/shard_map/branch_terms/pallas_call | solution.py:274
  50.2 15.7 %all_to_all.22.terms = bf16[8,16,2048]{2,1,0:T(8,128)(2,1)S(1)} all-to-all(bf16[8,16,2048]{2,1,0:T(8,128)(2,1)S(1)} %bitcast.16), channel_id=1, replica_groups={{0,8,16,24,32,40,48,56},{64,72,80,88,96,104,112,120},{128,136,144,152,1..., dimensions={0} | all-to-all | bytes 1048576 | tf_op jit(solution)/shard_map/all_to_all | solution.py:340
  65.9 0.1 collected.1
  66.0 15.2 %all_to_all.23.parts = bf16[32,2,2048]{2,1,0:T(2,128)(2,1)S(1)} all-to-all(bf16[32,2,2048]{2,1,0:T(2,128)(2,1)S(1)} %bitcast.17), channel_id=1, replica_groups={{0,1,2,3,64,65,66,67,128,129,130,131,192,193,194,195,256,257,258,259,32..., dimensions={0} | all-to-all | bytes 524288 | tf_op jit(solution)/shard_map/all_to_all | solution.py:345
  81.2 0.9 %last_norm.1 = bf16[2,512]{1,0:T(2,128)(2,1)} custom-call(bf16[32,2,2048]{2,1,0:T(2,128)(2,1)S(1)} %all_to_all.23.parts, bf16[8,16,2048]{2,1,0:T(8,128)(2,1)S(1)} %hidden_copies.1.hidden, f32[1,512]{1,0:T(1,128)S(1)} %get-tuple-element.21.gain, f32[1,512]{1,0:T(1,128)S(1)} %get-tuple-element.22.shift), custom_call_target="tpu_custom_call" | custom-call | tf_op jit(solution)/shard_map/last_norm/pallas_call | solution.py:317
Async XLA Ops:
  3.0 45.9 %collective-permute-start = (bf16[432,2048]{1,0:T(8,128)(2,1)S(1)}, bf16[432,2048]{1,0:T(8,128)(2,1)S(1)}, u32[]{:S(2)}, u32[]{:S(2)}) collective-permute-start(bf16[432,2048]{1,0:T(8,128)(2,1)S(1)} %get-tuple-element.18.mine), channel_id=1, source_target_pairs={{0,4},{4,0},{1,5},{5,1},{2,6},{6,2},{3,7},{7,3},{8,12},{12,8},{9,1... | collective-permute-start | bytes 5308424 | tf_op jit(solution)/shard_map/ppermute | solution.py:403
